TPU v7x, 32 devices: a whole 2x2x4 slice. The times are simulated.
32 devices in a mesh: ep: 8 (over z, x), tp: 4 (over y, core).
Axes of the slice: x: 2, y: 2, z: 4, core: 2. Of those that a mesh axis runs over, the one named last changes fastest.
Arguments:
- tokens: bfloat16 [4096, 2048], P(('ep', 'tp')), may hold values from -6 to 6
- routes: int32 [4096, 2], P(('ep', 'tp')), may hold values from 0 to 31, as said below
- gates: float32 [4096, 2], P(('ep', 'tp')), may hold values from 0.1 to 0.6
- w_gate: bfloat16 [32, 2048, 768], P(('ep', 'tp')), may hold values from -0.125 to 0.125
- w_up: bfloat16 [32, 2048, 768], P(('ep', 'tp')), may hold values from -0.125 to 0.125
- w_down: bfloat16 [32, 768, 2048], P(('ep', 'tp')), may hold values from -0.21875 to 0.21875
- moe_out: bfloat16 [4096, 2048], P('ep', 'tp'), may hold values from -16 to 16
- norm_gain: float32 [2048], P('tp'), may hold values from 0.1 to 1.9
- out_grad: bfloat16 [4096, 2048], P('ep', 'tp'), may hold values from -16 to 16
Outputs:
- token_grad: bfloat16 [4096, 2048], P(('ep', 'tp'))
- gates_grad: bfloat16 [4096, 2], P(('ep', 'tp'))
- w_gate_grad: bfloat16 [32, 2048, 768], P(('ep', 'tp'))
- w_up_grad: bfloat16 [32, 2048, 768], P(('ep', 'tp'))
- w_down_grad: bfloat16 [32, 768, 2048], P(('ep', 'tp'))
Inputs may be any that keep to these rules, and one draw needn't show every extreme that they name: `routes`: the two experts of a row differ and lie in one group (expert e is in group e // 8). In the 128 rows of one device the tokens fall into the groups in shares 3/8, 3/8, 1/8, 1/8 of 128, which group takes which share varying. In the rows of one device no expert is named more than 16 times, and one expert is named exactly 16 times in the rows of every device.
All inputs are finite; a program needn't handle non-finite values.
Results may differ from a plain program's by a relative error of at most 0.0071.
Values may be sent and summed in bfloat16 or wider, within the bound.
A program may use at most 128 MiB of HBM per device.

v0:
```python
import jax
import jax.numpy as jnp
from jax import lax
from jax.sharding import PartitionSpec as P

epsilon = 1e-06


def contract(left, right, left_dim, right_dim):
    return lax.dot_general(
        left, right, (((left_dim,), (right_dim,)), ((), ())), preferred_element_type=jnp.float32
    )


def slot_ranks(flat_ids, experts):
    one_hot = (flat_ids[:, None] == jnp.arange(experts, dtype=jnp.int32)[None, :]).astype(jnp.int32)
    return jnp.sum((jnp.cumsum(one_hot, axis=0) - one_hot) * one_hot, axis=1)


def local(tokens, routes, gates, w_gate, w_up, w_down, moe_out, norm_gain, out_grad):
    devices = lax.axis_size(("ep", "tp"))
    tok_rows, features = tokens.shape
    top_count = routes.shape[1]
    capacity = 4 * tok_rows // devices
    route_count = tok_rows * top_count
    saved_out = moe_out.astype(jnp.float32)
    scaled = norm_gain[None, :] * out_grad.astype(jnp.float32)
    square_sum, cross_sum = lax.psum(
        (jnp.sum(saved_out * saved_out, axis=1), jnp.sum(saved_out * scaled, axis=1)), "tp"
    )
    inv_rms = lax.rsqrt(square_sum / features + epsilon)
    expert_cot = (
        inv_rms[:, None] * scaled - saved_out * (inv_rms**3 * cross_sum / features)[:, None]
    ).astype(jnp.bfloat16)
    flat_ids = routes.reshape(-1)
    own_slots = flat_ids * capacity + slot_ranks(flat_ids, devices)
    route_tokens = jnp.arange(route_count, dtype=jnp.int32) // top_count
    token_of_slot = (
        jnp.full((devices * capacity,), tok_rows, jnp.int32).at[own_slots].set(route_tokens)
    )
    gate_slots = (
        jnp.zeros((devices * capacity,), jnp.bfloat16)
        .at[own_slots]
        .set(gates.reshape(-1).astype(jnp.bfloat16))
        .reshape(devices, capacity)
    )
    token_pad = jnp.concatenate([tokens, jnp.zeros((1, features), jnp.bfloat16)], axis=0)
    token_slots = token_pad[token_of_slot].reshape(devices, capacity, features)
    cot_rows = lax.all_to_all(expert_cot, "tp", split_axis=0, concat_axis=1, tiled=True)
    cot_pad = jnp.concatenate([cot_rows, jnp.zeros((1, features), jnp.bfloat16)], axis=0)
    cot_slots = cot_pad[token_of_slot].reshape(devices, capacity, features)
    token_in, cot_in, gate_in = (
        lax.all_to_all(token_slots, ("ep", "tp"), split_axis=0, concat_axis=0, tiled=True),
        lax.all_to_all(cot_slots, ("ep", "tp"), split_axis=0, concat_axis=0, tiled=True),
        lax.all_to_all(gate_slots, ("ep", "tp"), split_axis=0, concat_axis=0, tiled=True),
    )
    cot_in = cot_in.reshape(devices * capacity, features)
    row_block = token_in.reshape(devices * capacity, features)
    w_gate_one = w_gate[0]
    w_up_one = w_up[0]
    w_down_one = w_down[0]
    pre_gate = jnp.dot(row_block, w_gate_one, preferred_element_type=jnp.float32)
    pre_up = jnp.dot(row_block, w_up_one, preferred_element_type=jnp.float32)
    sigmoid_gate = jax.nn.sigmoid(pre_gate)
    activated = pre_gate * sigmoid_gate
    hidden = activated * pre_up
    hid_grad = contract(cot_in, w_down_one, 1, 1)
    gate_grad = jnp.sum(hidden * hid_grad, axis=1).astype(jnp.bfloat16)
    weight = gate_in.reshape(-1).astype(jnp.float32)[:, None]
    d_hidden = weight * hid_grad
    d_gate = (d_hidden * pre_up * sigmoid_gate * (1.0 + pre_gate * (1.0 - sigmoid_gate))).astype(
        jnp.bfloat16
    )
    d_up = (d_hidden * activated).astype(jnp.bfloat16)
    token_back = (contract(d_gate, w_gate_one, 1, 1) + contract(d_up, w_up_one, 1, 1)).astype(
        jnp.bfloat16
    )
    scaled_cot = (weight * cot_in.astype(jnp.float32)).astype(jnp.bfloat16)
    grad_gate = contract(row_block, d_gate, 0, 0).astype(jnp.bfloat16)
    grad_up = contract(row_block, d_up, 0, 0).astype(jnp.bfloat16)
    grad_down = contract(hidden.astype(jnp.bfloat16), scaled_cot, 0, 0).astype(jnp.bfloat16)
    back_rows, back_gates = (
        lax.all_to_all(
            token_back.reshape(devices, capacity, features),
            ("ep", "tp"),
            split_axis=0,
            concat_axis=0,
            tiled=True,
        ),
        lax.all_to_all(
            gate_grad.reshape(devices, capacity),
            ("ep", "tp"),
            split_axis=0,
            concat_axis=0,
            tiled=True,
        ),
    )
    per_route = back_rows.reshape(devices * capacity, features)[own_slots]
    token_grad = jnp.sum(
        per_route.astype(jnp.float32).reshape(tok_rows, top_count, features), axis=1
    ).astype(jnp.bfloat16)
    gates_grad = back_gates.reshape(-1)[own_slots].reshape(tok_rows, top_count)
    return (token_grad, gates_grad, grad_gate[None], grad_up[None], grad_down[None])


def solution(mesh):
    in_specs = (
        P(("ep", "tp"), None),
        P(("ep", "tp"), None),
        P(("ep", "tp"), None),
        P(("ep", "tp"), None, None),
        P(("ep", "tp"), None, None),
        P(("ep", "tp"), None, None),
        P("ep", "tp"),
        P("tp"),
        P("ep", "tp"),
    )
    out_specs = (
        P(("ep", "tp"), None),
        P(("ep", "tp"), None),
        P(("ep", "tp"), None, None),
        P(("ep", "tp"), None, None),
        P(("ep", "tp"), None, None),
    )
    return jax.shard_map(local, mesh=mesh, in_specs=in_specs, out_specs=out_specs, check_vma=False)
```

profile of v0, /device:TPU:0, one launch (start us, length us, event | category | flops | bytes accessed | tf_op | source)
XLA Modules:
  0.0 236.2 jit_solution(12114761283139347899)
XLA Ops:
  0.6 0.9 copy.23
  4.7 2.2 scatter_custom_fusion
  7.6 7.3 %all-to-all-start = ((bf16[32,1,16]{2,1,0:T(2,128)(2,1)}), bf16[32,1,16]{2,1,0:T(2,128)(2,1)S(1)}, u32[]{:S(2)}, u32[]{:S(2)}) async-start(bf16[32,1,16]{2,1,0:T(2,128)(2,1)} %all_to_all.43), calls=%async_computation | async-start | bytes 32768 | tf_op jit(solution)/shard_map/all_to_all | solution.py:55
  14.9 1.5 fusion.17
  16.4 7.2 %all-reduce.2 = (f32[512]{0:T(512)S(1)}, f32[512]{0:T(512)S(1)}) all-reduce(f32[512]{0:T(512)S(1)} %get-tuple-element.16, f32[512]{0:T(512)S(1)} %get-tuple-element.15), channel_id=1, replica_groups=mesh['ep'=8,'tp'=4] {'tp'}, use_global_device_ids=true, to_apply=%region_7.8 | all-reduce | flops 1024 | bytes 8192 | tf_op jit(solution)/shard_map/psum | solution.py:28
  23.6 2.3 fusion.20
  25.9 1.9 concatenate.7
  27.8 4.1 %all-to-all-start.1 = ((bf16[4,128,512]{2,1,0:T(8,128)(2,1)}), bf16[4,128,512]{2,1,0:T(8,128)(2,1)}, u32[]{:S(2)}, u32[]{:S(2)}) async-start(bf16[4,128,512]{2,1,0:T(8,128)(2,1)} %bitcast.66), calls=%async_computation.1 | async-start | bytes 1048576 | tf_op jit(solution)/shard_map/all_to_all | solution.py:49
  31.9 1.4 scatter_custom_fusion.1
  33.3 6.4 %gather_fusion.1 = bf16[512,2048]{1,0:T(8,128)(2,1)} fusion(bf16[129,2048]{1,0:T(8,128)(2,1)} %concatenate.7, s32[1024]{0:T(1024)S(1)} %pad_clamp_fusion.1), kind=kCustom, calls=%fused_computation.1 | custom fusion | bytes 4196352 | tf_op jit(solution)/shard_map/gather | solution.py:48
  39.7 1.1 all-to-all-done.1
  40.8 5.1 %all-to-all-start.3 = ((bf16[32,16,2048]{2,1,0:T(8,128)(2,1)}), bf16[32,16,2048]{2,1,0:T(8,128)(2,1)}, u32[]{:S(2)}, u32[]{:S(2)}) async-start(bf16[32,16,2048]{2,1,0:T(8,128)(2,1)} %bitcast.63), calls=%async_computation.3 | async-start | bytes 4194304 | tf_op jit(solution)/shard_map/all_to_all | solution.py:53
  45.9 1.1 copy.32
  47.8 6.3 %gather_fusion = bf16[512,2048]{1,0:T(8,128)(2,1)} fusion(bf16[129,2048]{1,0:T(8,128)(2,1)} %concatenate.6, s32[1024]{0:T(1024)S(1)} %pad_clamp_fusion.1), kind=kCustom, calls=%fused_computation | custom fusion | bytes 4196352 | tf_op jit(solution)/shard_map/gather | solution.py:51
  54.2 40.4 %all-to-all-done.3 = bf16[32,16,2048]{2,1,0:T(8,128)(2,1)} async-done(((bf16[32,16,2048]{2,1,0:T(8,128)(2,1)}), bf16[32,16,2048]{2,1,0:T(8,128)(2,1)}, u32[]{:S(2)}, u32[]{:S(2)}) %all-to-all-start.3) | async-done | bytes 2097184 | tf_op jit(solution)/shard_map/all_to_all | solution.py:53
  94.6 4.3 %all-to-all-start.2 = ((bf16[32,16,2048]{2,1,0:T(8,128)(2,1)}), bf16[32,16,2048]{2,1,0:T(8,128)(2,1)}, u32[]{:S(2)}, u32[]{:S(2)}) async-start(bf16[32,16,2048]{2,1,0:T(8,128)(2,1)} %bitcast.64), calls=%async_computation.2 | async-start | bytes 4194304 | tf_op jit(solution)/shard_map/all_to_all | solution.py:54
  99.0 4.7 %fusion.2 = f32[512,768]{1,0:T(8,128)} fusion(bf16[512,2048]{1,0:T(8,128)(2,1)} %bitcast.9, bf16[1,2048,768]{2,1,0:T(8,128)(2,1)S(1)} %copy-done), kind=kOutput, calls=%fused_computation.13 | convolution fusion | flops 1610612736 | bytes 6815744 | tf_op jit(solution)/shard_map/dot_general | solution.py:62
  103.7 4.6 %fusion.6 = f32[512,768]{1,0:T(8,128)} fusion(bf16[512,2048]{1,0:T(8,128)(2,1)} %bitcast.9, bf16[1,2048,768]{2,1,0:T(8,128)(2,1)S(1)} %copy-done.1), kind=kOutput, calls=%fused_computation.17 | convolution fusion | flops 1610612736 | bytes 6815744 | tf_op jit(solution)/shard_map/dot_general | solution.py:63
  108.3 39.1 %all-to-all-done.2 = bf16[32,16,2048]{2,1,0:T(8,128)(2,1)} async-done(((bf16[32,16,2048]{2,1,0:T(8,128)(2,1)}), bf16[32,16,2048]{2,1,0:T(8,128)(2,1)}, u32[]{:S(2)}, u32[]{:S(2)}) %all-to-all-start.2) | async-done | bytes 2097184 | tf_op jit(solution)/shard_map/all_to_all | solution.py:54
  147.4 6.7 %multiply_reduce_fusion = (bf16[512]{0:T(512)(128)(2,1)S(1)}, bf16[512,768]{1,0:T(8,128)(2,1)S(1)}, bf16[512,768]{1,0:T(8,128)(2,1)}) fusion(f32[512,768]{1,0:T(8,128)} %fusion.6, f32[512,768]{1,0:T(8,128)} %fusion.2, f32[512]{0:T(512)S(1)} %reshape.128, bf16[512,2048]{1,0:T(8,128)(2,1)} %bitcast.6, bf16[1,768,2048]{2,1,0:T(8,128)(2,1)} %param.14), kind=kOutput, calls=%fused_computation.25 | convolution fusion | flops 1617296896 | bytes 9964544 | tf_op jit(solution)/shard_map/dot_general | solution.py:10
  154.2 3.8 %fusion = f32[512,2048]{1,0:T(8,128)} fusion(bf16[512,768]{1,0:T(8,128)(2,1)S(1)} %get-tuple-element.20, bf16[1,2048,768]{2,1,0:T(8,128)(2,1)S(1)} %copy-done), kind=kOutput, calls=%fused_computation.11 | convolution fusion | flops 1610612736 | bytes 8126464 | tf_op jit(solution)/shard_map/dot_general | solution.py:10
  158.6 4.0 %all-to-all-start.5 = ((bf16[32,1,16]{2,1,0:T(2,128)(2,1)}), bf16[32,1,16]{2,1,0:T(2,128)(2,1)S(1)}, u32[]{:S(2)}, u32[]{:S(2)}) async-start(bf16[32,1,16]{2,1,0:T(2,128)(2,1)} %convert_element_type.97), calls=%async_computation.5 | async-start | bytes 32768 | tf_op jit(solution)/shard_map/all_to_all | solution.py:90
  162.6 6.6 %add_convert_fusion = bf16[512,2048]{1,0:T(8,128)(2,1)} fusion(f32[512,2048]{1,0:T(8,128)} %fusion, bf16[512,768]{1,0:T(8,128)(2,1)} %get-tuple-element.21, bf16[1,2048,768]{2,1,0:T(8,128)(2,1)} %param.13), kind=kOutput, calls=%fused_computation.7 | convolution fusion | flops 1612709888 | bytes 10223616 | tf_op jit(solution)/shard_map/dot_general | solution.py:10
  169.7 5.7 %all-to-all-start.4 = ((bf16[32,16,2048]{2,1,0:T(8,128)(2,1)}), bf16[32,16,2048]{2,1,0:T(8,128)(2,1)}, u32[]{:S(2)}, u32[]{:S(2)}) async-start(bf16[32,16,2048]{2,1,0:T(8,128)(2,1)} %bitcast.65), calls=%async_computation.4 | async-start | bytes 4194304 | tf_op jit(solution)/shard_map/all_to_all | solution.py:83
  175.5 5.3 %fusion.10 = bf16[1,2048,768]{2,1,0:T(8,128)(2,1)} fusion(bf16[512,2048]{1,0:T(8,128)(2,1)} %bitcast.9, bf16[512,768]{1,0:T(8,128)(2,1)} %copy-done.3), kind=kOutput, calls=%fused_computation.21 | convolution fusion | flops 1612185600 | bytes 6029312 | tf_op jit(solution)/shard_map/dot_general | solution.py:10
  180.8 5.2 %fusion.11 = bf16[1,2048,768]{2,1,0:T(8,128)(2,1)} fusion(bf16[512,2048]{1,0:T(8,128)(2,1)} %bitcast.9, bf16[512,768]{1,0:T(8,128)(2,1)S(1)} %copy-done.2), kind=kOutput, calls=%fused_computation.22 | convolution fusion | flops 1612185600 | bytes 6029312 | tf_op jit(solution)/shard_map/dot_general | solution.py:10
  186.1 5.3 %fusion.12 = bf16[1,768,2048]{2,1,0:T(8,128)(2,1)} fusion(bf16[512,2048]{1,0:T(8,128)(2,1)} %bitcast.6, f32[512]{0:T(512)S(1)} %reshape.128, f32[512,768]{1,0:T(8,128)S(1)} %copy-done.5, f32[512,768]{1,0:T(8,128)S(1)} %copy-done.4), kind=kOutput, calls=%fused_computation.23 | convolution fusion | flops 1617690624 | bytes 8390656 | tf_op jit(solution)/shard_map/dot_general | solution.py:10
  191.5 1.9 gather_fusion.3
  194.2 29.7 %all-to-all-done.4 = bf16[32,16,2048]{2,1,0:T(8,128)(2,1)} async-done(((bf16[32,16,2048]{2,1,0:T(8,128)(2,1)}), bf16[32,16,2048]{2,1,0:T(8,128)(2,1)}, u32[]{:S(2)}, u32[]{:S(2)}) %all-to-all-start.4) | async-done | bytes 2097184 | tf_op jit(solution)/shard_map/all_to_all | solution.py:83
  223.9 5.2 %gather_fusion.2 = bf16[256,2048]{1,0:T(8,128)(2,1)} fusion(bf16[512,2048]{1,0:T(8,128)(2,1)} %bitcast.13, s32[1024]{0:T(1024)S(1)} %pad_clamp_fusion), kind=kCustom, calls=%fused_computation.2 | custom fusion | bytes 2098176 | tf_op jit(solution)/shard_map/gather | solution.py:98
  229.1 2.5 %gather.17 = bf16[128,2,2048]{2,1,0:T(2,128)(2,1)} reshape(bf16[256,2048]{1,0:T(8,128)(2,1)} %gather_fusion.2) | data formatting | bytes 2097152 | tf_op jit(solution)/shard_map/gather | solution.py:98
  231.7 4.6 %reduce_sum.54 = bf16[128,2048]{1,0:T(8,128)(2,1)} reduce(bf16[128,2,2048]{2,1,0:T(2,128)(2,1)} %gather.17, bf16[]{:T(256)} %constant.17.clone.1), dimensions={1}, to_apply=%region_9.10 | reduce | flops 262144 | bytes 1572866 | tf_op jit(solution)/shard_map/reduce_sum | solution.py:99
  (43 shorter events, 7.0 us)
Async XLA Ops:
  0.6 98.4 %copy-start = (bf16[1,2048,768]{2,1,0:T(8,128)(2,1)S(1)}, bf16[1,2048,768]{2,1,0:T(8,128)(2,1)}, u32[]{:S(2)}) copy-start(bf16[1,2048,768]{2,1,0:T(8,128)(2,1)} %param.12) | copy-start | bytes 9437188
  7.6 20.2 %all-to-all-start = ((bf16[32,1,16]{2,1,0:T(2,128)(2,1)}), bf16[32,1,16]{2,1,0:T(2,128)(2,1)S(1)}, u32[]{:S(2)}, u32[]{:S(2)}) async-start(bf16[32,1,16]{2,1,0:T(2,128)(2,1)} %all_to_all.43), calls=%async_computation | async-start | bytes 32768 | tf_op jit(solution)/shard_map/all_to_all | solution.py:55
  27.8 13.0 %all-to-all-start.1 = ((bf16[4,128,512]{2,1,0:T(8,128)(2,1)}), bf16[4,128,512]{2,1,0:T(8,128)(2,1)}, u32[]{:S(2)}, u32[]{:S(2)}) async-start(bf16[4,128,512]{2,1,0:T(8,128)(2,1)} %bitcast.66), calls=%async_computation.1 | async-start | bytes 1048576 | tf_op jit(solution)/shard_map/all_to_all | solution.py:49
  40.8 53.8 %all-to-all-start.3 = ((bf16[32,16,2048]{2,1,0:T(8,128)(2,1)}), bf16[32,16,2048]{2,1,0:T(8,128)(2,1)}, u32[]{:S(2)}, u32[]{:S(2)}) async-start(bf16[32,16,2048]{2,1,0:T(8,128)(2,1)} %bitcast.63), calls=%async_computation.3 | async-start | bytes 4194304 | tf_op jit(solution)/shard_map/all_to_all | solution.py:53
  94.6 52.8 %all-to-all-start.2 = ((bf16[32,16,2048]{2,1,0:T(8,128)(2,1)}), bf16[32,16,2048]{2,1,0:T(8,128)(2,1)}, u32[]{:S(2)}, u32[]{:S(2)}) async-start(bf16[32,16,2048]{2,1,0:T(8,128)(2,1)} %bitcast.64), calls=%async_computation.2 | async-start | bytes 4194304 | tf_op jit(solution)/shard_map/all_to_all | solution.py:54
  99.0 4.7 %copy-start.1 = (bf16[1,2048,768]{2,1,0:T(8,128)(2,1)S(1)}, bf16[1,2048,768]{2,1,0:T(8,128)(2,1)}, u32[]{:S(2)}) copy-start(bf16[1,2048,768]{2,1,0:T(8,128)(2,1)} %param.13) | copy-start | bytes 9437188
  154.2 3.8 %copy-start.3 = (bf16[512,768]{1,0:T(8,128)(2,1)}, bf16[512,768]{1,0:T(8,128)(2,1)S(1)}, u32[]{:S(2)}) copy-start(bf16[512,768]{1,0:T(8,128)(2,1)S(1)} %get-tuple-element.20) | copy-start | bytes 2359300
  158.6 11.1 %all-to-all-start.5 = ((bf16[32,1,16]{2,1,0:T(2,128)(2,1)}), bf16[32,1,16]{2,1,0:T(2,128)(2,1)S(1)}, u32[]{:S(2)}, u32[]{:S(2)}) async-start(bf16[32,1,16]{2,1,0:T(2,128)(2,1)} %convert_element_type.97), calls=%async_computation.5 | async-start | bytes 32768 | tf_op jit(solution)/shard_map/all_to_all | solution.py:90
  169.7 54.2 %all-to-all-start.4 = ((bf16[32,16,2048]{2,1,0:T(8,128)(2,1)}), bf16[32,16,2048]{2,1,0:T(8,128)(2,1)}, u32[]{:S(2)}, u32[]{:S(2)}) async-start(bf16[32,16,2048]{2,1,0:T(8,128)(2,1)} %bitcast.65), calls=%async_computation.4 | async-start | bytes 4194304 | tf_op jit(solution)/shard_map/all_to_all | solution.py:83
  175.5 5.4 %copy-start.2 = (bf16[512,768]{1,0:T(8,128)(2,1)S(1)}, bf16[512,768]{1,0:T(8,128)(2,1)}, u32[]{:S(2)}) copy-start(bf16[512,768]{1,0:T(8,128)(2,1)} %get-tuple-element.21) | copy-start | bytes 2359300
  180.8 5.3 %copy-start.4 = (f32[512,768]{1,0:T(8,128)S(1)}, f32[512,768]{1,0:T(8,128)}, u32[]{:S(2)}) copy-start(f32[512,768]{1,0:T(8,128)} %fusion.2) | copy-start | bytes 4718596
  180.8 5.3 %copy-start.5 = (f32[512,768]{1,0:T(8,128)S(1)}, f32[512,768]{1,0:T(8,128)}, u32[]{:S(2)}) copy-start(f32[512,768]{1,0:T(8,128)} %fusion.6) | copy-start | bytes 4718596
where the time goes:
time: 237 us; the launch traced here: 236 us
  waiting for transfers between devices  111 us (47%)
  matrix products  42.2 us (18%)
  local copies, waits for them, and re-layouts  34.1 us (14%)
  starting transfers between devices  30.6 us (13%)
  other arithmetic  10.6 us (4%)
  blocking collectives  7.15 us (3%)
    all_to_all x1, waiting for transfers between devices, local(): lax.all_to_all(token_slots, ('ep', 'tp'), split_axis=0, concat_axis=0, ti...  40.4 us
    all_to_all x1, waiting for transfers between devices, local(): lax.all_to_all(cot_slots, ('ep', 'tp'), split_axis=0, concat_axis=0, tile...  39.1 us
    dot_general x6, matrix products, contract(): lax.dot_general(left, right, (((left_dim,), (right_dim,)), ((), ())), pre...  33 us
    all_to_all x1, waiting for transfers between devices, local(): lax.all_to_all(token_back.reshape(devices, capacity, features), ('ep', 't...  29.7 us
    gather x2, local copies, waits for them, and re-layouts, local(): per_route = back_rows.reshape(devices * capacity, features)[own_slots]  7.75 us
    all_to_all x1, starting transfers between devices, local(): lax.all_to_all(gate_slots, ('ep', 'tp'), split_axis=0, concat_axis=0, til...  7.33 us
    psum x1, blocking collectives, local(): lax.psum((jnp.sum(saved_out * saved_out, axis=1), jnp.sum(saved_out * sca...  7.15 us
    gather x1, local copies, waits for them, and re-layouts, local(): token_slots = token_pad[token_of_slot].reshape(devices, capacity, features)  6.35 us
  transfers between devices with their start and end apart: 6, of which 5 were waited for; matrix products, arithmetic and copies ran while one was open for 24% of the time, Pallas kernels for 0%

commit v1 on v0

v1 whole, which is shorter than its diff:
```python
import functools

import jax
import jax.numpy as jnp
from jax import lax
from jax.experimental import pallas as pl
from jax.experimental.pallas import tpu as pltpu
from jax.sharding import Mesh
from jax.sharding import PartitionSpec as P

epsilon = 1e-06
groups = 4
MESH = pl.DeviceIdType.MESH
AXES = ("z", "x", "tp")


def contract(left, right, left_dim, right_dim):
    return lax.dot_general(
        left, right, (((left_dim,), (right_dim,)), ((), ())), preferred_element_type=jnp.float32
    )


def earlier_equal(ids):
    count = ids.shape[-1]
    place = jnp.arange(count, dtype=jnp.int32)
    same = (ids[..., :, None] == ids[..., None, :]) & (place[:, None] > place[None, :])
    return jnp.sum(same.astype(jnp.int32), axis=-1)


def places(plane_size):
    z, x, t = (lax.axis_index(name) for name in AXES)
    z_count, t_count = lax.axis_size("z"), lax.axis_size("tp")
    own = x * t_count + t

    def z_peer(d):
        return (lax.rem(z + d, z_count), x, t)

    def plane_peer(k):
        q = lax.rem(own + k, plane_size)
        return q, (z, q // t_count, lax.rem(q, t_count))

    return z, own, z_count, z_peer, plane_peer


def enter(z_count, plane_size, z_peer, plane_peer):
    barrier = pltpu.get_barrier_semaphore()
    for d in range(1, z_count):
        pl.semaphore_signal(barrier, inc=1, device_id=z_peer(d), device_id_type=MESH)

    def greet(k, carry):
        pl.semaphore_signal(barrier, inc=1, device_id=plane_peer(k)[1], device_id_type=MESH)
        return carry

    lax.fori_loop(1, plane_size, greet, 0)
    pl.semaphore_wait(barrier, z_count - 1 + plane_size - 1)


def columns_dot(left, read, write, features):
    chunk = min(512, features)

    def one(c, carry):
        cols = pl.ds(pl.multiple_of(c * chunk, chunk), chunk)
        write(cols, jnp.dot(left, read(cols), preferred_element_type=jnp.float32))
        return carry

    lax.fori_loop(0, features // chunk, one, 0)


def dispatch_kernel(
    plane_size, slots, tok_ref, cot_ref, sel_ref, tok_out, cot_out,
    zbuf, sbuf, zs_sem, zr_sem, ps_sem, pr_sem, loc_sem,
):
    z, own, z_count, z_peer, plane_peer = places(plane_size)
    features = tok_ref.shape[-1]
    sends, outs = (tok_ref, cot_ref), (tok_out, cot_out)
    enter(z_count, plane_size, z_peer, plane_peer)

    def z_copy(a, d):
        return pltpu.make_async_remote_copy(
            src_ref=sends[a].at[lax.rem(z + d, z_count)],
            dst_ref=zbuf.at[a, d],
            send_sem=zs_sem.at[a, d],
            recv_sem=zr_sem.at[a, d],
            device_id=z_peer(d),
            device_id_type=MESH,
        )

    def rows_of(q):
        return pl.ds(pl.multiple_of(q * slots, slots), slots)

    def plane_copy(a, d, k):
        q, device = plane_peer(k)
        src = lax.rem(z + z_count - d, z_count)
        return pltpu.make_async_remote_copy(
            src_ref=sbuf.at[a, d, rows_of(q)],
            dst_ref=outs[a].at[src, rows_of(own)],
            send_sem=ps_sem.at[a, d, k],
            recv_sem=pr_sem.at[a, d, k],
            device_id=device,
            device_id_type=MESH,
        )

    def own_copy(a, d):
        src = lax.rem(z + z_count - d, z_count)
        return pltpu.make_async_copy(
            sbuf.at[a, d, rows_of(own)], outs[a].at[src, rows_of(own)], loc_sem.at[a, d]
        )

    for a in range(2):
        for d in range(1, z_count):
            z_copy(a, d).start()
    for a, d in [(0, 0), (1, 0)] + [(a, d) for a in range(2) for d in range(1, z_count)]:
        src = lax.rem(z + z_count - d, z_count)
        if d:
            z_copy(a, d).wait_recv()

        def read(cols):
            return zbuf[a, d, :, cols] if d else sends[a][z, :, cols]

        def write(cols, value):
            sbuf[a, d, :, cols] = value.astype(sbuf.dtype)

        columns_dot(sel_ref[src], read, write, features)
        lax.fori_loop(1, plane_size, lambda k, c: (plane_copy(a, d, k).start(), c)[1], 0)
        own_copy(a, d).start()
    for a in range(2):
        for d in range(z_count):
            if d:
                z_copy(a, d).wait_send()
            own_copy(a, d).wait()
            lax.fori_loop(1, plane_size, lambda k, c: (plane_copy(a, d, k).wait(), c)[1], 0)


def combine_kernel(
    plane_size, slots, back_ref, comb_ref, out_ref,
    rbuf, cbuf, zs_sem, zr_sem, ps_sem, pr_sem, loc_sem, own_sem,
):
    z, own, z_count, z_peer, plane_peer = places(plane_size)
    features = back_ref.shape[-1]
    enter(z_count, plane_size, z_peer, plane_peer)

    def rows_of(q):
        return pl.ds(pl.multiple_of(q * slots, slots), slots)

    def plane_copy(d, k):
        q, device = plane_peer(k)
        return pltpu.make_async_remote_copy(
            src_ref=back_ref.at[lax.rem(z + d, z_count), rows_of(q)],
            dst_ref=rbuf.at[d, rows_of(own)],
            send_sem=ps_sem.at[d, k],
            recv_sem=pr_sem.at[d, k],
            device_id=device,
            device_id_type=MESH,
        )

    def own_rows(d):
        return pltpu.make_async_copy(
            back_ref.at[lax.rem(z + d, z_count), rows_of(own)], rbuf.at[d, rows_of(own)], loc_sem.at[d]
        )

    def z_copy(d):
        return pltpu.make_async_remote_copy(
            src_ref=cbuf.at[d],
            dst_ref=out_ref.at[z],
            send_sem=zs_sem.at[d],
            recv_sem=zr_sem.at[d],
            device_id=z_peer(d),
            device_id_type=MESH,
        )

    keep = pltpu.make_async_copy(cbuf.at[0], out_ref.at[z], own_sem)
    order = list(range(1, z_count)) + [0]
    for d in order:
        own_rows(d).start()
        lax.fori_loop(1, plane_size, lambda k, c: (plane_copy(d, k).start(), c)[1], 0)
    for d in order:
        own_rows(d).wait()
        lax.fori_loop(1, plane_size, lambda k, c: (plane_copy(d, k).wait_recv(), c)[1], 0)

        def read(cols):
            return rbuf[d, :, cols]

        def write(cols, value):
            cbuf[d, :, cols] = value.astype(cbuf.dtype)

        columns_dot(comb_ref[lax.rem(z + d, z_count)], read, write, features)
        if d:
            z_copy(d).start()
        else:
            keep.start()
    for d in order:
        lax.fori_loop(1, plane_size, lambda k, c: (plane_copy(d, k).wait_send(), c)[1], 0)
        if d:
            z_copy(d).wait()
    keep.wait()


def dispatch(tok_send, cot_send, select, plane_size, slots):
    z_count, rows, features = tok_send.shape
    out = jax.ShapeDtypeStruct((z_count, plane_size * slots, features), tok_send.dtype)
    vmem, any_space = pl.BlockSpec(memory_space=pltpu.VMEM), pl.BlockSpec(memory_space=pl.ANY)
    dma = pltpu.SemaphoreType.DMA
    return pl.pallas_call(
        functools.partial(dispatch_kernel, plane_size, slots),
        out_shape=(out, out),
        in_specs=[vmem] * 3,
        out_specs=(any_space, any_space),
        scratch_shapes=[
            pltpu.VMEM((2, z_count, rows, features), tok_send.dtype),
            pltpu.VMEM((2,) + out.shape, tok_send.dtype),
            dma((2, z_count)),
            dma((2, z_count)),
            dma((2, z_count, plane_size)),
            dma((2, z_count, plane_size)),
            dma((2, z_count)),
        ],
        compiler_params=pltpu.CompilerParams(
            collective_id=0, has_side_effects=True, vmem_limit_bytes=48 * 1024 * 1024
        ),
        name="dispatch",
    )(tok_send, cot_send, select)


def combine(back, comb, plane_size, slots):
    z_count, _, features = back.shape
    rows = comb.shape[1]
    vmem, any_space = pl.BlockSpec(memory_space=pltpu.VMEM), pl.BlockSpec(memory_space=pl.ANY)
    dma = pltpu.SemaphoreType.DMA
    return pl.pallas_call(
        functools.partial(combine_kernel, plane_size, slots),
        out_shape=jax.ShapeDtypeStruct((z_count, rows, features), back.dtype),
        in_specs=[any_space, vmem],
        out_specs=any_space,
        scratch_shapes=[
            pltpu.VMEM(back.shape, back.dtype),
            pltpu.VMEM((z_count, rows, features), back.dtype),
            dma((z_count,)),
            dma((z_count,)),
            dma((z_count, plane_size)),
            dma((z_count, plane_size)),
            dma((z_count,)),
            dma(()),
        ],
        compiler_params=pltpu.CompilerParams(
            collective_id=1, has_side_effects=True, vmem_limit_bytes=48 * 1024 * 1024
        ),
        name="combine",
    )(back, comb)


def local(tokens, routes, gates, w_gate, w_up, w_down, moe_out, norm_gain, out_grad):
    z_count, x_count, t_count = (lax.axis_size(name) for name in AXES)
    plane_size = x_count * t_count
    devices = z_count * plane_size
    z, x, t = (lax.axis_index(name) for name in AXES)
    own = x * t_count + t
    me = z * plane_size + own
    tok_rows, features = tokens.shape
    top_count = routes.shape[1]
    capacity = groups * tok_rows // devices
    slots = -(-capacity // 16) * 16
    group_rows = 3 * tok_rows // 8
    route_count = tok_rows * top_count
    bf16 = jnp.bfloat16

    saved_out = moe_out.astype(jnp.float32)
    scaled = norm_gain[None, :] * out_grad.astype(jnp.float32)
    stats = jnp.stack([jnp.sum(saved_out * saved_out, axis=1), jnp.sum(saved_out * scaled, axis=1)])
    packed = jnp.concatenate(
        [stats.reshape(-1), routes.T.reshape(-1).astype(jnp.float32), gates.T.reshape(-1)]
    )
    gathered = lax.all_gather(packed, AXES, axis=0, tiled=False)
    stat_count = stats.size
    ep_stats = lax.dynamic_slice(gathered, (me - t, 0), (t_count, stat_count))
    square_sum, cross_sum = jnp.sum(ep_stats.reshape(t_count, 2, -1), axis=0)
    all_ids = gathered[:, stat_count : stat_count + route_count].astype(jnp.int32)
    all_gates = gathered[:, stat_count + route_count :].astype(bf16).astype(jnp.float32)

    inv_rms = lax.rsqrt(square_sum / features + epsilon)
    expert_cot = (
        inv_rms[:, None] * scaled - saved_out * (inv_rms**3 * cross_sum / features)[:, None]
    ).astype(bf16)
    cot_rows = lax.all_to_all(expert_cot, "tp", split_axis=0, concat_axis=1, tiled=True)

    own_ids = routes.T.reshape(-1)
    own_group = routes[:, 0] // plane_size
    z_slot = own_group * group_rows + earlier_equal(own_group)
    pack = (jnp.arange(groups * group_rows, dtype=jnp.int32)[:, None] == z_slot[None, :]).astype(bf16)
    tok_send = jnp.dot(pack, tokens, preferred_element_type=jnp.float32).astype(bf16)
    cot_send = jnp.dot(pack, cot_rows, preferred_element_type=jnp.float32).astype(bf16)

    ids = lax.dynamic_index_in_dim(
        all_ids.reshape(z_count, plane_size, route_count), own, axis=1, keepdims=False
    )
    slot_of = (ids - z * plane_size) * slots + earlier_equal(ids)
    slot_of = jnp.where(ids // plane_size == z, slot_of, -1)
    group_of = ids[:, :tok_rows] // plane_size
    row_of = jnp.where(group_of == z, earlier_equal(group_of), -1)
    row_of = jnp.tile(row_of, (1, top_count))
    at_slot = (
        slot_of[:, None, :] == jnp.arange(plane_size * slots, dtype=jnp.int32)[None, :, None]
    ).astype(bf16)
    at_row = (row_of[:, None, :] == jnp.arange(group_rows, dtype=jnp.int32)[None, :, None]).astype(bf16)
    select = jnp.einsum("zsf,zrf->zsr", at_slot, at_row, preferred_element_type=jnp.float32).astype(bf16)
    spread = jnp.einsum("zrf,zsf->zrs", at_row, at_slot, preferred_element_type=jnp.float32).astype(bf16)

    hit = all_ids == me
    hit_rank = jnp.cumsum(hit.astype(jnp.int32), axis=1) - 1
    chosen = hit[:, None, :] & (
        hit_rank[:, None, :] == jnp.arange(slots, dtype=jnp.int32)[None, :, None]
    )
    weight = jnp.sum(jnp.where(chosen, all_gates[:, None, :], 0.0), axis=2).reshape(-1)[:, None]

    token_in, cot_in = dispatch(
        tok_send.reshape(groups, group_rows, features),
        cot_send.reshape(groups, group_rows, features),
        select,
        plane_size,
        slots,
    )
    row_block = token_in.reshape(devices * slots, features)
    cot_in = cot_in.reshape(devices * slots, features)
    w_gate_one = w_gate[0]
    w_up_one = w_up[0]
    w_down_one = w_down[0]
    pre_gate = jnp.dot(row_block, w_gate_one, preferred_element_type=jnp.float32)
    pre_up = jnp.dot(row_block, w_up_one, preferred_element_type=jnp.float32)
    sigmoid_gate = jax.nn.sigmoid(pre_gate)
    activated = pre_gate * sigmoid_gate
    hidden = activated * pre_up
    hid_grad = contract(cot_in, w_down_one, 1, 1)
    gate_grad = jnp.sum(hidden * hid_grad, axis=1).astype(bf16)
    d_hidden = weight * hid_grad
    d_gate = (d_hidden * pre_up * sigmoid_gate * (1.0 + pre_gate * (1.0 - sigmoid_gate))).astype(bf16)
    d_up = (d_hidden * activated).astype(bf16)
    token_back = (contract(d_gate, w_gate_one, 1, 1) + contract(d_up, w_up_one, 1, 1)).astype(bf16)
    scaled_cot = (weight * cot_in.astype(jnp.float32)).astype(bf16)
    grad_gate = contract(row_block, d_gate, 0, 0).astype(bf16)
    grad_up = contract(row_block, d_up, 0, 0).astype(bf16)
    grad_down = contract(hidden.astype(bf16), scaled_cot, 0, 0).astype(bf16)

    back_gates = lax.all_to_all(
        gate_grad.reshape(devices, slots), AXES, split_axis=0, concat_axis=0, tiled=True
    )
    back = combine(
        token_back.reshape(z_count, plane_size * slots, features), spread, plane_size, slots
    )
    token_grad = contract(pack, back.reshape(groups * group_rows, features), 0, 0).astype(bf16)
    own_slots = own_ids * slots + earlier_equal(own_ids)
    picked = own_slots[:, None] == jnp.arange(devices * slots, dtype=jnp.int32)[None, :]
    gates_grad = jnp.sum(
        jnp.where(picked, back_gates.reshape(1, -1).astype(jnp.float32), 0.0), axis=1
    ).astype(bf16)
    gates_grad = gates_grad.reshape(top_count, tok_rows).T
    return (token_grad, gates_grad, grad_gate[None], grad_up[None], grad_down[None])


def solution(mesh):
    ep, tp = mesh.shape["ep"], mesh.shape["tp"]
    cut = Mesh(mesh.devices.reshape(groups, ep // groups, tp), AXES)
    rows, ep_axes = P(AXES, None), ("z", "x")
    cube = P(AXES, None, None)
    return jax.shard_map(
        local,
        mesh=cut,
        in_specs=(rows, rows, rows, cube, cube, cube, P(ep_axes, "tp"), P("tp"), P(ep_axes, "tp")),
        out_specs=(rows, rows, cube, cube, cube),
        check_vma=False,
    )
```

time: 237 us -> 187 us (0.79)
  waiting for transfers between devices: 111 us -> 0.01 us
  Pallas kernels: 0 us -> 82.4 us
  blocking collectives: 7.15 us -> 43.8 us
  local copies, waits for them, and re-layouts: 34.1 us -> 6.82 us
  starting transfers between devices: 30.6 us -> 11.6 us
  matrix products: 42.2 us -> 29.2 us
    all_to_all x5 -> x1, waiting for transfers between devices: 110 us -> 0.01 us  [local(): lax.all_to_all(gate_grad.reshape(devices, slots), AXES, split_axis=0, con...]
    pallas_call x0 -> x2, Pallas kernels: none -> 82.4 us  [the longest x1 49.8 us: dispatch(): pl.pallas_call(functools.partial(dispatch_kernel, plane_size, slots), out...]
    all_gather x0 -> x1, blocking collectives: none -> 43.8 us  [local(): gathered = lax.all_gather(packed, AXES, axis=0, tiled=False)]
    gather x5 -> x0, local copies, waits for them, and re-layouts: 22.4 us -> none  [the longest x2 7.75 us: local(): per_route = back_rows.reshape(devices * capacity, features)[own_slots]]
    all_to_all x5 -> x1, starting transfers between devices: 26.4 us -> 7.47 us  [local(): lax.all_to_all(gate_grad.reshape(devices, slots), AXES, split_axis=0, con...]
    dot_general x6 -> x7, matrix products: 33 us -> 19.6 us  [contract(): lax.dot_general(left, right, (((left_dim,), (right_dim,)), ((), ())), pre...]
    psum x1 -> x0, blocking collectives: 7.15 us -> none  [local(): lax.psum((jnp.sum(saved_out * saved_out, axis=1), jnp.sum(saved_out * sca...]
    dot_general x0 -> x4, matrix products: none -> 4.14 us  [the longest x1 2.28 us: local(): jnp.dot(pack, tokens, preferred_element_type=jnp.float32).astype(bf16)]
  transfers between devices with their start and end apart: 6 -> 2, of which waited for: 5 -> 0; matrix products, arithmetic and copies ran while one was open for 24% -> 5% of each run, Pallas kernels for 0% -> 17%
where the time goes in v1:
time: 187 us; the launch traced here: 186 us
  Pallas kernels  82.4 us (44%)
  blocking collectives  43.8 us (23%)
  matrix products  29.2 us (16%)
  starting transfers between devices  11.6 us (6%)
  other arithmetic  11.4 us (6%)
  local copies, waits for them, and re-layouts  6.82 us (4%)
    pallas_call x1, Pallas kernels, dispatch(): pl.pallas_call(functools.partial(dispatch_kernel, plane_size, slots), out...  49.8 us
    all_gather x1, blocking collectives, local(): gathered = lax.all_gather(packed, AXES, axis=0, tiled=False)  43.8 us
    pallas_call x1, Pallas kernels, combine(): pl.pallas_call(functools.partial(combine_kernel, plane_size, slots), out_...  32.6 us
    dot_general x7, matrix products, contract(): lax.dot_general(left, right, (((left_dim,), (right_dim,)), ((), ())), pre...  19.6 us
    all_to_all x1, starting transfers between devices, local(): lax.all_to_all(gate_grad.reshape(devices, slots), AXES, split_axis=0, con...  7.47 us
    all_to_all x1, starting transfers between devices, local(): lax.all_to_all(expert_cot, 'tp', split_axis=0, concat_axis=1, tiled=True)  4.13 us
  transfers between devices with their start and end apart: 2, of which 0 were waited for; matrix products, arithmetic and copies ran while one was open for 5% of the time, Pallas kernels for 17%

profile of v1, /device:TPU:0, one launch (start us, length us, event | category | flops | bytes accessed | tf_op | source)
XLA Modules:
  0.0 186.1 jit_solution(15363641608972613387)
XLA Ops:
  0.7 0.8 bitcast_convert_fusion
  1.5 1.6 fusion.17
  3.2 0.7 pad_maximum_fusion
  3.9 43.8 %all-gather.1 = f32[32,1,1536]{2,1,0:T(1,128)S(1)} all-gather(f32[1,1,1536]{2,1,0:T(1,128)S(1)} %reshape.220), channel_id=2, replica_groups=mesh['z'=4,'x'=2,'tp'=4] {'z','x','tp'}, dimensions={0}, use_global_device_ids=true | all-gather | bytes 202752 | tf_op jit(solution)/shard_map/all_gather | solution.py:272
  47.7 2.3 %fusion.20 = bf16[512,512]{1,0:T(8,128)(2,1)} fusion(bf16[512,512]{1,0:T(8,128)(2,1)} %param.15, bf16[512,512]{1,0:T(8,128)(2,1)} %param.17, f32[512]{0:T(512)S(1)} %get-tuple-element.17, f32[512]{0:T(512)S(1)} %get-tuple-element.16, f32[512]{0:T(512)} %param.16), kind=kLoop, calls=%fused_computation.35 | loop fusion | flops 1835008 | bytes 1579008 | tf_op jit(solution)/shard_map/convert_element_type | solution.py:282
  49.9 4.1 %all-to-all-start = ((bf16[4,128,512]{2,1,0:T(8,128)(2,1)}), bf16[4,128,512]{2,1,0:T(8,128)(2,1)}, u32[]{:S(2)}, u32[]{:S(2)}) async-start(bf16[4,128,512]{2,1,0:T(8,128)(2,1)} %bitcast.116), calls=%async_computation | async-start | bytes 1048576 | tf_op jit(solution)/shard_map/all_to_all | solution.py:283
  54.1 0.5 fusion.43
  54.7 0.6 fusion.33
  55.3 0.6 convert_bitcast_fusion
  57.3 0.8 copy.52
  58.0 0.6 reduce-window.6
  58.9 1.0 select_reduce_fusion.1
  60.1 0.8 convert_reduce_fusion.3
  61.0 2.3 %convolution_convert_fusion.4 = bf16[192,2048]{1,0:T(8,128)(2,1)} fusion(bf16[128,2048]{1,0:T(8,128)(2,1)} %param.9, s32[128]{0:T(128)S(1)} %multiply_add_fusion.1), kind=kOutput, calls=%fused_computation.19 | convolution fusion | flops 101081088 | bytes 1311232 | tf_op jit(solution)/shard_map/dot_general | solution.py:289
  63.3 2.0 %copy.35 = bf16[128,4,512]{0,2,1:T(8,128)(2,1)} copy(bf16[128,4,512]{2,0,1:T(8,128)(2,1)} %bitcast.10) | data formatting | bytes 1048576 | tf_op jit(solution)/shard_map/all_to_all | solution.py:283
  65.3 1.4 convolution_convert_fusion.3
  66.8 1.1 copy-done.1
  67.9 49.8 %dispatch.1 = (bf16[4,128,2048]{2,1,0:T(8,128)(2,1)S(1)}, bf16[4,128,2048]{2,1,0:T(8,128)(2,1)S(1)}) custom-call(bf16[4,48,2048]{2,1,0:T(8,128)(2,1)S(1)} %bitcast.105, bf16[4,48,2048]{2,1,0:T(8,128)(2,1)S(1)} %bitcast.106, bf16[4,128,48]{2,1,0:T(8,128)(2,1)S(1)} %copy.37.sel_ref), custom_call_target="tpu_custom_call" | custom-call | tf_op jit(solution)/shard_map/dispatch/pallas_call | solution.py:203
  117.7 3.7 %fusion.6 = f32[512,768]{1,0:T(8,128)S(1)} fusion(bf16[512,2048]{1,0:T(8,128)(2,1)S(1)} %bitcast.109, bf16[1,2048,768]{2,1,0:T(8,128)(2,1)} %param.13), kind=kOutput, calls=%fused_computation.11 | convolution fusion | flops 1610612736 | bytes 6815744 | tf_op jit(solution)/shard_map/dot_general | solution.py:327
  121.4 1.8 fusion.2
  123.3 2.5 %multiply_reduce_fusion = (bf16[512]{0:T(512)(128)(2,1)S(1)}, bf16[512,768]{1,0:T(8,128)(2,1)S(1)}, bf16[512,768]{1,0:T(8,128)(2,1)S(1)}) fusion(f32[512,768]{1,0:T(8,128)S(1)} %fusion.6, f32[512,768]{1,0:T(8,128)S(1)} %fusion.2, f32[512]{0:T(512)S(1)} %mul.119, bf16[512,2048]{1,0:T(8,128)(2,1)S(1)} %bitcast.113, bf16[1,768,2048]{2,1,0:T(8,128)(2,1)S(1)} %copy-done.4), kind=kOutput, calls=%fused_computation.22 | convolution fusion | flops 1617296896 | bytes 9964544 | tf_op jit(solution)/shard_map/dot_general | solution.py:18
  125.8 1.8 fusion
  127.6 3.5 %fusion.10 = bf16[1,2048,768]{2,1,0:T(8,128)(2,1)} fusion(bf16[512,2048]{1,0:T(8,128)(2,1)S(1)} %bitcast.111, bf16[512,768]{1,0:T(8,128)(2,1)S(1)} %get-tuple-element.14), kind=kOutput, calls=%fused_computation.15 | convolution fusion | flops 1612185600 | bytes 6029312 | tf_op jit(solution)/shard_map/dot_general | solution.py:18
  131.1 3.7 %fusion.12 = bf16[1,768,2048]{2,1,0:T(8,128)(2,1)} fusion(bf16[512,2048]{1,0:T(8,128)(2,1)S(1)} %bitcast.114, f32[512]{0:T(512)S(1)} %mul.119, f32[512,768]{1,0:T(8,128)S(1)} %fusion.6, f32[512,768]{1,0:T(8,128)S(1)} %fusion.2), kind=kOutput, calls=%fused_computation.17 | convolution fusion | flops 1617690624 | bytes 8390656 | tf_op jit(solution)/shard_map/dot_general | solution.py:18
  134.8 3.7 %fusion.11 = bf16[1,2048,768]{2,1,0:T(8,128)(2,1)} fusion(bf16[512,2048]{1,0:T(8,128)(2,1)S(1)} %bitcast.112, bf16[512,768]{1,0:T(8,128)(2,1)S(1)} %get-tuple-element.15), kind=kOutput, calls=%fused_computation.16 | convolution fusion | flops 1612185600 | bytes 6029312 | tf_op jit(solution)/shard_map/dot_general | solution.py:18
  138.6 3.2 %add_convert_fusion = bf16[512,2048]{1,0:T(8,128)(2,1)} fusion(f32[512,2048]{1,0:T(8,128)S(1)} %fusion, bf16[512,768]{1,0:T(8,128)(2,1)S(1)} %get-tuple-element.15, bf16[1,2048,768]{2,1,0:T(8,128)(2,1)S(1)} %copy-done.5), kind=kOutput, calls=%fused_computation.1 | convolution fusion | flops 1612709888 | bytes 10223616 | tf_op jit(solution)/shard_map/dot_general | solution.py:18
  141.7 0.7 convert_element_type.140
  142.4 7.5 %all-to-all-start.1 = ((bf16[32,1,16]{2,1,0:T(2,128)(2,1)}), bf16[32,1,16]{2,1,0:T(2,128)(2,1)S(1)}, u32[]{:S(2)}, u32[]{:S(2)}) async-start(bf16[32,1,16]{2,1,0:T(2,128)(2,1)} %convert_element_type.140), calls=%async_computation.1 | async-start | bytes 32768 | tf_op jit(solution)/shard_map/all_to_all | solution.py:342
  149.9 1.6 copy-done.2
  151.5 32.6 %combine.1 = bf16[4,48,2048]{2,1,0:T(8,128)(2,1)S(1)} custom-call(bf16[4,128,2048]{2,1,0:T(8,128)(2,1)S(1)} %bitcast.108, bf16[4,48,128]{2,1,0:T(8,128)(2,1)S(1)} %convolution_convert_fusion.6.comb_ref), custom_call_target="tpu_custom_call" | custom-call | tf_op jit(solution)/shard_map/combine/pallas_call | solution.py:229
  184.1 1.1 convolution_convert_fusion.5
  185.3 0.7 select_reduce_fusion
  (44 shorter events, 2.2 us)
Async XLA Ops:
  0.6 120.8 %copy-start = (bf16[1,2048,768]{2,1,0:T(8,128)(2,1)S(1)}, bf16[1,2048,768]{2,1,0:T(8,128)(2,1)}, u32[]{:S(2)}) copy-start(bf16[1,2048,768]{2,1,0:T(8,128)(2,1)} %param.12) | copy-start | bytes 9437188
  0.6 53.4 %copy-start.3 = (s32[128,2]{0,1:T(2,128)S(1)}, s32[128,2]{0,1:T(2,128)}, u32[]{:S(2)}) copy-start(s32[128,2]{0,1:T(2,128)} %param.10) | copy-start | bytes 3076
  49.9 13.3 %all-to-all-start = ((bf16[4,128,512]{2,1,0:T(8,128)(2,1)}), bf16[4,128,512]{2,1,0:T(8,128)(2,1)}, u32[]{:S(2)}, u32[]{:S(2)}) async-start(bf16[4,128,512]{2,1,0:T(8,128)(2,1)} %bitcast.116), calls=%async_computation | async-start | bytes 1048576 | tf_op jit(solution)/shard_map/all_to_all | solution.py:283
  66.8 1.1 copy-start.1
  121.4 1.9 %copy-start.4 = (bf16[1,768,2048]{2,1,0:T(8,128)(2,1)S(1)}, bf16[1,768,2048]{2,1,0:T(8,128)(2,1)}, u32[]{:S(2)}) copy-start(bf16[1,768,2048]{2,1,0:T(8,128)(2,1)} %param.14) | copy-start | bytes 9437188
  134.8 3.7 %copy-start.5 = (bf16[1,2048,768]{2,1,0:T(8,128)(2,1)S(1)}, bf16[1,2048,768]{2,1,0:T(8,128)(2,1)}, u32[]{:S(2)}) copy-start(bf16[1,2048,768]{2,1,0:T(8,128)(2,1)} %param.13) | copy-start | bytes 9437188
  142.4 42.8 %all-to-all-start.1 = ((bf16[32,1,16]{2,1,0:T(2,128)(2,1)}), bf16[32,1,16]{2,1,0:T(2,128)(2,1)S(1)}, u32[]{:S(2)}, u32[]{:S(2)}) async-start(bf16[32,1,16]{2,1,0:T(2,128)(2,1)} %convert_element_type.140), calls=%async_computation.1 | async-start | bytes 32768 | tf_op jit(solution)/shard_map/all_to_all | solution.py:342
  149.9 1.6 copy-start.2

commit v2 on v1

--- a/solution.py
+++ b/solution.py
@@ -132,67 +132,138 @@
 
 
 def combine_kernel(
-    plane_size, slots, back_ref, comb_ref, out_ref,
-    rbuf, cbuf, zs_sem, zr_sem, ps_sem, pr_sem, loc_sem, own_sem,
+    plane_size, slots, back_ref, gate_ref, comb_ref, out_ref, gate_out,
+    rbuf, gbuf, cbuf, hbuf, zs_sem, zr_sem, ps_sem, pr_sem, loc_sem, own_sem,
 ):
     z, own, z_count, z_peer, plane_peer = places(plane_size)
-    features = back_ref.shape[-1]
+    sources, landed, sums, outs = (gate_ref, back_ref), (gbuf, rbuf), (hbuf, cbuf), (gate_out, out_ref)
     enter(z_count, plane_size, z_peer, plane_peer)
 
     def rows_of(q):
         return pl.ds(pl.multiple_of(q * slots, slots), slots)
 
-    def plane_copy(d, k):
+    def plane_copy(a, d, k):
         q, device = plane_peer(k)
         return pltpu.make_async_remote_copy(
-            src_ref=back_ref.at[lax.rem(z + d, z_count), rows_of(q)],
-            dst_ref=rbuf.at[d, rows_of(own)],
-            send_sem=ps_sem.at[d, k],
-            recv_sem=pr_sem.at[d, k],
+            src_ref=sources[a].at[lax.rem(z + d, z_count), rows_of(q)],
+            dst_ref=landed[a].at[d, rows_of(own)],
+            send_sem=ps_sem.at[a, d, k],
+            recv_sem=pr_sem.at[a, d, k],
             device_id=device,
             device_id_type=MESH,
         )
 
-    def own_rows(d):
+    def own_rows(a, d):
         return pltpu.make_async_copy(
-            back_ref.at[lax.rem(z + d, z_count), rows_of(own)], rbuf.at[d, rows_of(own)], loc_sem.at[d]
-        )
-
-    def z_copy(d):
-        return pltpu.make_async_remote_copy(
-            src_ref=cbuf.at[d],
-            dst_ref=out_ref.at[z],
-            send_sem=zs_sem.at[d],
-            recv_sem=zr_sem.at[d],
+            sources[a].at[lax.rem(z + d, z_count), rows_of(own)],
+            landed[a].at[d, rows_of(own)],
+            loc_sem.at[a, d],
+        )
+
+    def z_copy(a, d):
+        return pltpu.make_async_remote_copy(
+            src_ref=sums[a].at[d],
+            dst_ref=outs[a].at[z],
+            send_sem=zs_sem.at[a, d],
+            recv_sem=zr_sem.at[a, d],
             device_id=z_peer(d),
             device_id_type=MESH,
         )
 
-    keep = pltpu.make_async_copy(cbuf.at[0], out_ref.at[z], own_sem)
+    keep = [pltpu.make_async_copy(sums[a].at[0], outs[a].at[z], own_sem.at[a]) for a in range(2)]
     order = list(range(1, z_count)) + [0]
     for d in order:
-        own_rows(d).start()
-        lax.fori_loop(1, plane_size, lambda k, c: (plane_copy(d, k).start(), c)[1], 0)
+        for a in range(2):
+            own_rows(a, d).start()
+            lax.fori_loop(1, plane_size, lambda k, c: (plane_copy(a, d, k).start(), c)[1], 0)
     for d in order:
-        own_rows(d).wait()
-        lax.fori_loop(1, plane_size, lambda k, c: (plane_copy(d, k).wait_recv(), c)[1], 0)
-
-        def read(cols):
-            return rbuf[d, :, cols]
-
-        def write(cols, value):
-            cbuf[d, :, cols] = value.astype(cbuf.dtype)
-
-        columns_dot(comb_ref[lax.rem(z + d, z_count)], read, write, features)
-        if d:
-            z_copy(d).start()
-        else:
-            keep.start()
+        for a in range(2):
+            own_rows(a, d).wait()
+            lax.fori_loop(1, plane_size, lambda k, c: (plane_copy(a, d, k).wait_recv(), c)[1], 0)
+
+            def read(cols):
+                return landed[a][d, :, cols]
+
+            def write(cols, value):
+                sums[a][d, :, cols] = value.astype(sums[a].dtype)
+
+            columns_dot(comb_ref[lax.rem(z + d, z_count)], read, write, landed[a].shape[-1])
+            if d:
+                z_copy(a, d).start()
+            else:
+                keep[a].start()
     for d in order:
-        lax.fori_loop(1, plane_size, lambda k, c: (plane_copy(d, k).wait_send(), c)[1], 0)
-        if d:
-            z_copy(d).wait()
-    keep.wait()
+        for a in range(2):
+            lax.fori_loop(1, plane_size, lambda k, c: (plane_copy(a, d, k).wait_send(), c)[1], 0)
+            if d:
+                z_copy(a, d).wait()
+            else:
+                keep[a].wait()
+
+
+def share_kernel(devices, stat_ref, meta_ref, stat_out, meta_out, ss_sem, sr_sem, ms_sem, mr_sem):
+    z, x, t = (lax.axis_index(name) for name in AXES)
+    x_count, t_count = lax.axis_size("x"), lax.axis_size("tp")
+    me = (z * x_count + x) * t_count + t
+
+    def peer(k):
+        q = lax.rem(me + k, devices)
+        return (q // (x_count * t_count), lax.rem(q // t_count, x_count), lax.rem(q, t_count))
+
+    def meta_copy(k):
+        return pltpu.make_async_remote_copy(
+            src_ref=meta_ref,
+            dst_ref=meta_out.at[me],
+            send_sem=ms_sem.at[k],
+            recv_sem=mr_sem.at[k],
+            device_id=peer(k),
+            device_id_type=MESH,
+        )
+
+    def stat_copy(j):
+        return pltpu.make_async_remote_copy(
+            src_ref=stat_ref,
+            dst_ref=stat_out.at[t],
+            send_sem=ss_sem.at[j],
+            recv_sem=sr_sem.at[j],
+            device_id=(z, x, lax.rem(t + j, t_count)),
+            device_id_type=MESH,
+        )
+
+    barrier = pltpu.get_barrier_semaphore()
+
+    def greet(k, carry):
+        pl.semaphore_signal(barrier, inc=1, device_id=peer(k), device_id_type=MESH)
+        return carry
+
+    lax.fori_loop(1, devices, greet, 0)
+    pl.semaphore_wait(barrier, devices - 1)
+    for j in range(1, t_count):
+        stat_copy(j).start()
+    lax.fori_loop(1, devices, lambda k, c: (meta_copy(k).start(), c)[1], 0)
+    stat_out[t] = stat_ref[...]
+    meta_out[me] = meta_ref[...]
+    for j in range(1, t_count):
+        stat_copy(j).wait()
+    lax.fori_loop(1, devices, lambda k, c: (meta_copy(k).wait(), c)[1], 0)
+
+
+def share(stats, meta, devices):
+    vmem = pl.BlockSpec(memory_space=pltpu.VMEM)
+    t_count = lax.axis_size("tp")
+    dma = pltpu.SemaphoreType.DMA
+    return pl.pallas_call(
+        functools.partial(share_kernel, devices),
+        out_shape=(
+            jax.ShapeDtypeStruct((t_count,) + stats.shape, stats.dtype),
+            jax.ShapeDtypeStruct((devices,) + meta.shape, meta.dtype),
+        ),
+        in_specs=[vmem] * 2,
+        out_specs=(vmem, vmem),
+        scratch_shapes=[dma((t_count,)), dma((t_count,)), dma((devices,)), dma((devices,))],
+        compiler_params=pltpu.CompilerParams(collective_id=2, has_side_effects=True),
+        name="share",
+    )(stats, meta)
 
 
 def dispatch(tok_send, cot_send, select, plane_size, slots):
@@ -221,31 +292,36 @@
     )(tok_send, cot_send, select)
 
 
-def combine(back, comb, plane_size, slots):
+def combine(back, gate_back, comb, plane_size, slots):
     z_count, _, features = back.shape
-    rows = comb.shape[1]
+    rows, lanes = comb.shape[1], gate_back.shape[-1]
     vmem, any_space = pl.BlockSpec(memory_space=pltpu.VMEM), pl.BlockSpec(memory_space=pl.ANY)
     dma = pltpu.SemaphoreType.DMA
     return pl.pallas_call(
         functools.partial(combine_kernel, plane_size, slots),
-        out_shape=jax.ShapeDtypeStruct((z_count, rows, features), back.dtype),
-        in_specs=[any_space, vmem],
-        out_specs=any_space,
+        out_shape=(
+            jax.ShapeDtypeStruct((z_count, rows, features), back.dtype),
+            jax.ShapeDtypeStruct((z_count, rows, lanes), back.dtype),
+        ),
+        in_specs=[any_space, any_space, vmem],
+        out_specs=(any_space, any_space),
         scratch_shapes=[
             pltpu.VMEM(back.shape, back.dtype),
+            pltpu.VMEM(gate_back.shape, back.dtype),
             pltpu.VMEM((z_count, rows, features), back.dtype),
-            dma((z_count,)),
-            dma((z_count,)),
-            dma((z_count, plane_size)),
-            dma((z_count, plane_size)),
-            dma((z_count,)),
-            dma(()),
+            pltpu.VMEM((z_count, rows, lanes), back.dtype),
+            dma((2, z_count)),
+            dma((2, z_count)),
+            dma((2, z_count, plane_size)),
+            dma((2, z_count, plane_size)),
+            dma((2, z_count)),
+            dma((2,)),
         ],
         compiler_params=pltpu.CompilerParams(
             collective_id=1, has_side_effects=True, vmem_limit_bytes=48 * 1024 * 1024
         ),
         name="combine",
-    )(back, comb)
+    )(back, gate_back, comb)
 
 
 def local(tokens, routes, gates, w_gate, w_up, w_down, moe_out, norm_gain, out_grad):
@@ -262,19 +338,17 @@
     group_rows = 3 * tok_rows // 8
     route_count = tok_rows * top_count
     bf16 = jnp.bfloat16
+    lanes = 128
 
     saved_out = moe_out.astype(jnp.float32)
     scaled = norm_gain[None, :] * out_grad.astype(jnp.float32)
     stats = jnp.stack([jnp.sum(saved_out * saved_out, axis=1), jnp.sum(saved_out * scaled, axis=1)])
-    packed = jnp.concatenate(
-        [stats.reshape(-1), routes.T.reshape(-1).astype(jnp.float32), gates.T.reshape(-1)]
-    )
-    gathered = lax.all_gather(packed, AXES, axis=0, tiled=False)
-    stat_count = stats.size
-    ep_stats = lax.dynamic_slice(gathered, (me - t, 0), (t_count, stat_count))
-    square_sum, cross_sum = jnp.sum(ep_stats.reshape(t_count, 2, -1), axis=0)
-    all_ids = gathered[:, stat_count : stat_count + route_count].astype(jnp.int32)
-    all_gates = gathered[:, stat_count + route_count :].astype(bf16).astype(jnp.float32)
+    meta = jnp.concatenate([routes.T.astype(jnp.float32), gates.T], axis=0).reshape(-1, lanes)
+    all_stats, all_meta = share(stats.reshape(-1, lanes), meta, devices)
+    square_sum, cross_sum = jnp.sum(all_stats.reshape(t_count, 2, -1), axis=0)
+    all_meta = all_meta.reshape(devices, 2 * route_count)
+    all_ids = all_meta[:, :route_count].astype(jnp.int32)
+    all_gates = lax.reduce_precision(all_meta[:, route_count:], 8, 7)
 
     inv_rms = lax.rsqrt(square_sum / features + epsilon)
     expert_cot = (
@@ -282,7 +356,6 @@
     ).astype(bf16)
     cot_rows = lax.all_to_all(expert_cot, "tp", split_axis=0, concat_axis=1, tiled=True)
 
-    own_ids = routes.T.reshape(-1)
     own_group = routes[:, 0] // plane_size
     z_slot = own_group * group_rows + earlier_equal(own_group)
     pack = (jnp.arange(groups * group_rows, dtype=jnp.int32)[:, None] == z_slot[None, :]).astype(bf16)
@@ -310,6 +383,8 @@
         hit_rank[:, None, :] == jnp.arange(slots, dtype=jnp.int32)[None, :, None]
     )
     weight = jnp.sum(jnp.where(chosen, all_gates[:, None, :], 0.0), axis=2).reshape(-1)[:, None]
+    column = jnp.arange(route_count, dtype=jnp.int32) // tok_rows
+    which = jnp.sum(jnp.where(chosen, column[None, None, :], 0), axis=2).reshape(-1)
 
     token_in, cot_in = dispatch(
         tok_send.reshape(groups, group_rows, features),
@@ -339,19 +414,19 @@
     grad_up = contract(row_block, d_up, 0, 0).astype(bf16)
     grad_down = contract(hidden.astype(bf16), scaled_cot, 0, 0).astype(bf16)
 
-    back_gates = lax.all_to_all(
-        gate_grad.reshape(devices, slots), AXES, split_axis=0, concat_axis=0, tiled=True
-    )
-    back = combine(
-        token_back.reshape(z_count, plane_size * slots, features), spread, plane_size, slots
+    gate_back = jnp.where(
+        jnp.arange(lanes, dtype=jnp.int32)[None, :] == which[:, None], gate_grad[:, None], 0
+    ).astype(bf16)
+    back, gate_sums = combine(
+        token_back.reshape(z_count, plane_size * slots, features),
+        gate_back.reshape(z_count, plane_size * slots, lanes),
+        spread,
+        plane_size,
+        slots,
     )
     token_grad = contract(pack, back.reshape(groups * group_rows, features), 0, 0).astype(bf16)
-    own_slots = own_ids * slots + earlier_equal(own_ids)
-    picked = own_slots[:, None] == jnp.arange(devices * slots, dtype=jnp.int32)[None, :]
-    gates_grad = jnp.sum(
-        jnp.where(picked, back_gates.reshape(1, -1).astype(jnp.float32), 0.0), axis=1
-    ).astype(bf16)
-    gates_grad = gates_grad.reshape(top_count, tok_rows).T
+    gates_grad = contract(pack, gate_sums.reshape(groups * group_rows, lanes), 0, 0).astype(bf16)
+    gates_grad = gates_grad[:, :top_count]
     return (token_grad, gates_grad, grad_gate[None], grad_up[None], grad_down[None])
 
 

time: 187 us -> 150 us (0.80)
  blocking collectives: 43.8 us -> 0 us
  Pallas kernels: 82.4 us -> 98.6 us
  starting transfers between devices: 11.6 us -> 4.13 us
  waiting for transfers between devices: 0.01 us -> 2.97 us
  other arithmetic: 11.4 us -> 9.34 us
  local copies, waits for them, and re-layouts: 6.82 us -> 4.9 us
    all_gather x1 -> x0, blocking collectives: 43.8 us -> none  [local(): gathered = lax.all_gather(packed, AXES, axis=0, tiled=False)]
    pallas_call x0 -> x1, Pallas kernels: none -> 11.6 us  [share(): pl.pallas_call(functools.partial(share_kernel, devices), out_shape=(jax.S...]
    all_to_all x1 -> x0, starting transfers between devices: 7.47 us -> none  [local(): lax.all_to_all(gate_grad.reshape(devices, slots), AXES, split_axis=0, con...]
    pallas_call x1, Pallas kernels: 32.6 us -> 36.5 us  [combine(): pl.pallas_call(functools.partial(combine_kernel, plane_size, slots), out_...]
    all_to_all x1, waiting for transfers between devices: 0.01 us -> 2.97 us  [local(): lax.all_to_all(expert_cot, 'tp', split_axis=0, concat_axis=1, tiled=True)]
    dot_general x7 -> x8, matrix products: 19.6 us -> 18.4 us  [contract(): lax.dot_general(left, right, (((left_dim,), (right_dim,)), ((), ())), pre...]
  transfers between devices with their start and end apart: 2 -> 1, of which waited for: 0 -> 1; matrix products, arithmetic and copies ran while one was open for 5% -> 4% of each run, Pallas kernels for 17% -> 0%
where the time goes in v2:
time: 150 us; the launch traced here: 149 us
  Pallas kernels  98.6 us (66%)
  matrix products  28 us (19%)
  other arithmetic  9.34 us (6%)
  local copies, waits for them, and re-layouts  4.9 us (3%)
  starting transfers between devices  4.13 us (3%)
  waiting for transfers between devices  2.97 us (2%)
    pallas_call x1, Pallas kernels, dispatch(): pl.pallas_call(functools.partial(dispatch_kernel, plane_size, slots), out...  50.5 us
    pallas_call x1, Pallas kernels, combine(): pl.pallas_call(functools.partial(combine_kernel, plane_size, slots), out_...  36.5 us
    dot_general x8, matrix products, contract(): lax.dot_general(left, right, (((left_dim,), (right_dim,)), ((), ())), pre...  18.4 us
    pallas_call x1, Pallas kernels, share(): pl.pallas_call(functools.partial(share_kernel, devices), out_shape=(jax.S...  11.6 us
    all_to_all x1, starting transfers between devices, local(): lax.all_to_all(expert_cot, 'tp', split_axis=0, concat_axis=1, tiled=True)  4.13 us
    dot_general x1, matrix products, local(): pre_up = jnp.dot(row_block, w_up_one, preferred_element_type=jnp.float32)  3.67 us
  transfers between devices with their start and end apart: 1, of which 1 were waited for; matrix products, arithmetic and copies ran while one was open for 4% of the time, Pallas kernels for 0%

profile of v2, /device:TPU:0, one launch (start us, length us, event | category | flops | bytes accessed | tf_op | source)
XLA Modules:
  0.0 149.0 jit_solution(3144817094051543987)
XLA Ops:
  0.7 1.7 %fusion.17 = (f32[512]{0:T(512)S(1)}, f32[512]{0:T(512)S(1)}) fusion(bf16[512,512]{1,0:T(8,128)(2,1)} %param.15, bf16[512,512]{1,0:T(8,128)(2,1)} %param.17, f32[512]{0:T(512)} %param.16), kind=kLoop, calls=%fused_computation.32 | loop fusion | flops 1833984 | bytes 1054720 | tf_op jit(solution)/shard_map/reduce_sum | solution.py:345
  2.3 0.6 reshape.209.stat_ref
  2.9 0.7 convert_bitcast_fusion.2
  3.6 1.3 pad_maximum_fusion.1.meta_ref
  4.9 11.6 %share.1 = (f32[4,8,128]{2,1,0:T(8,128)}, f32[32,4,128]{2,1,0:T(4,128)}) custom-call(f32[8,128]{1,0:T(8,128)} %reshape.209.stat_ref, f32[4,128]{1,0:T(4,128)} %pad_maximum_fusion.1.meta_ref), custom_call_target="tpu_custom_call" | custom-call | tf_op jit(solution)/shard_map/share/pallas_call | solution.py:255
  16.5 0.8 reduce_sum.87
  17.3 2.3 %fusion.20 = bf16[512,512]{1,0:T(8,128)(2,1)} fusion(bf16[512,512]{1,0:T(8,128)(2,1)} %param.15, bf16[512,512]{1,0:T(8,128)(2,1)} %param.17, f32[512]{0:T(512)S(1)} %fusion.42, f32[512]{0:T(512)S(1)} %rsqrt_bitcast_fusion, f32[512]{0:T(512)} %param.16), kind=kLoop, calls=%fused_computation.35 | loop fusion | flops 1835008 | bytes 1579008 | tf_op jit(solution)/shard_map/convert_element_type | solution.py:356
  19.6 4.1 %all-to-all-start = ((bf16[4,128,512]{2,1,0:T(8,128)(2,1)}), bf16[4,128,512]{2,1,0:T(8,128)(2,1)}, u32[]{:S(2)}, u32[]{:S(2)}) async-start(bf16[4,128,512]{2,1,0:T(8,128)(2,1)} %bitcast.116), calls=%async_computation | async-start | bytes 1048576 | tf_op jit(solution)/shard_map/all_to_all | solution.py:357
  23.9 0.4 convert_reduce_fusion
  24.3 0.2 convert_reduce_fusion.1
  24.6 0.2 convolution_convert_fusion.7
  24.9 0.2 convolution_convert_fusion.6.comb_ref
  25.3 0.6 reduce-window.6
  26.4 0.6 select_reduce_fusion
  27.3 2.3 %convolution_convert_fusion.4 = bf16[192,2048]{1,0:T(8,128)(2,1)} fusion(bf16[128,2048]{1,0:T(8,128)(2,1)} %param.9, s32[128]{0:T(128)S(1)} %multiply_add_fusion), kind=kOutput, calls=%fused_computation.19 | convolution fusion | flops 101081088 | bytes 1311232 | tf_op jit(solution)/shard_map/dot_general | solution.py:362
  29.6 3.0 %all-to-all-done = bf16[4,128,512]{2,1,0:T(8,128)(2,1)} async-done(((bf16[4,128,512]{2,1,0:T(8,128)(2,1)}), bf16[4,128,512]{2,1,0:T(8,128)(2,1)}, u32[]{:S(2)}, u32[]{:S(2)}) %all-to-all-start) | async-done | bytes 524320 | tf_op jit(solution)/shard_map/all_to_all | solution.py:357
  32.6 2.0 %copy.34 = bf16[128,4,512]{0,2,1:T(8,128)(2,1)} copy(bf16[128,4,512]{2,0,1:T(8,128)(2,1)} %bitcast.10) | data formatting | bytes 1048576 | tf_op jit(solution)/shard_map/all_to_all | solution.py:357
  34.6 1.4 convolution_convert_fusion.3
  36.1 1.1 copy-done.1
  37.2 50.5 %dispatch.1 = (bf16[4,128,2048]{2,1,0:T(8,128)(2,1)S(1)}, bf16[4,128,2048]{2,1,0:T(8,128)(2,1)S(1)}) custom-call(bf16[4,48,2048]{2,1,0:T(8,128)(2,1)S(1)} %bitcast.104, bf16[4,48,2048]{2,1,0:T(8,128)(2,1)S(1)} %bitcast.105, bf16[4,128,48]{2,1,0:T(8,128)(2,1)S(1)} %copy.36.sel_ref), custom_call_target="tpu_custom_call" | custom-call | tf_op jit(solution)/shard_map/dispatch/pallas_call | solution.py:274
  87.7 3.7 %fusion.6 = f32[512,768]{1,0:T(8,128)S(1)} fusion(bf16[512,2048]{1,0:T(8,128)(2,1)S(1)} %bitcast.108, bf16[1,2048,768]{2,1,0:T(8,128)(2,1)} %param.13), kind=kOutput, calls=%fused_computation.11 | convolution fusion | flops 1610612736 | bytes 6815744 | tf_op jit(solution)/shard_map/dot_general | solution.py:402
  91.4 1.8 %fusion.2 = f32[512,768]{1,0:T(8,128)S(1)} fusion(bf16[512,2048]{1,0:T(8,128)(2,1)S(1)} %bitcast.109, bf16[1,2048,768]{2,1,0:T(8,128)(2,1)S(1)} %copy-done), kind=kOutput, calls=%fused_computation.7 | convolution fusion | flops 1610612736 | bytes 6815744 | tf_op jit(solution)/shard_map/dot_general | solution.py:401
  93.3 2.5 %multiply_reduce_fusion = (bf16[512]{0:T(512)(128)(2,1)S(1)}, bf16[512,768]{1,0:T(8,128)(2,1)S(1)}, bf16[512,768]{1,0:T(8,128)(2,1)S(1)}) fusion(f32[512,768]{1,0:T(8,128)S(1)} %fusion.6, f32[512,768]{1,0:T(8,128)S(1)} %fusion.2, f32[512]{0:T(512)S(1)} %mul.111, bf16[512,2048]{1,0:T(8,128)(2,1)S(1)} %bitcast.112, bf16[1,768,2048]{2,1,0:T(8,128)(2,1)S(1)} %copy-done.4), kind=kOutput, calls=%fused_computation.22 | convolution fusion | flops 1617296896 | bytes 9964544 | tf_op jit(solution)/shard_map/dot_general | solution.py:18
  95.8 1.8 %fusion = f32[512,2048]{1,0:T(8,128)S(1)} fusion(bf16[512,768]{1,0:T(8,128)(2,1)S(1)} %get-tuple-element.22, bf16[1,2048,768]{2,1,0:T(8,128)(2,1)S(1)} %copy-done), kind=kOutput, calls=%fused_computation.5 | convolution fusion | flops 1610612736 | bytes 8126464 | tf_op jit(solution)/shard_map/dot_general | solution.py:18
  97.6 3.5 %fusion.10 = bf16[1,2048,768]{2,1,0:T(8,128)(2,1)} fusion(bf16[512,2048]{1,0:T(8,128)(2,1)S(1)} %bitcast.110, bf16[512,768]{1,0:T(8,128)(2,1)S(1)} %get-tuple-element.22), kind=kOutput, calls=%fused_computation.15 | convolution fusion | flops 1612185600 | bytes 6029312 | tf_op jit(solution)/shard_map/dot_general | solution.py:18
  101.1 3.7 %fusion.12 = bf16[1,768,2048]{2,1,0:T(8,128)(2,1)} fusion(bf16[512,2048]{1,0:T(8,128)(2,1)S(1)} %bitcast.113, f32[512]{0:T(512)S(1)} %mul.111, f32[512,768]{1,0:T(8,128)S(1)} %fusion.6, f32[512,768]{1,0:T(8,128)S(1)} %fusion.2), kind=kOutput, calls=%fused_computation.17 | convolution fusion | flops 1617690624 | bytes 8390656 | tf_op jit(solution)/shard_map/dot_general | solution.py:18
  104.8 3.7 %fusion.11 = bf16[1,2048,768]{2,1,0:T(8,128)(2,1)} fusion(bf16[512,2048]{1,0:T(8,128)(2,1)S(1)} %bitcast.111, bf16[512,768]{1,0:T(8,128)(2,1)S(1)} %get-tuple-element.23), kind=kOutput, calls=%fused_computation.16 | convolution fusion | flops 1612185600 | bytes 6029312 | tf_op jit(solution)/shard_map/dot_general | solution.py:18
  108.5 1.8 %add_convert_fusion = bf16[512,2048]{1,0:T(8,128)(2,1)S(1)} fusion(f32[512,2048]{1,0:T(8,128)S(1)} %fusion, bf16[512,768]{1,0:T(8,128)(2,1)S(1)} %get-tuple-element.23, bf16[1,2048,768]{2,1,0:T(8,128)(2,1)S(1)} %copy-done.5), kind=kOutput, calls=%fused_computation.1 | convolution fusion | flops 1612709888 | bytes 10223616 | tf_op jit(solution)/shard_map/dot_general | solution.py:18
  110.6 36.5 %combine.1 = (bf16[4,48,2048]{2,1,0:T(8,128)(2,1)S(1)}, bf16[4,48,128]{2,1,0:T(8,128)(2,1)S(1)}) custom-call(bf16[4,128,2048]{2,1,0:T(8,128)(2,1)S(1)} %bitcast.106, bf16[4,128,128]{2,1,0:T(8,128)(2,1)S(1)} %fusion.26.gate_ref, bf16[4,48,128]{2,1,0:T(8,128)(2,1)S(1)} %convolution_convert_fusion.6.comb_ref), custom_call_target="tpu_custom_call" | custom-call | tf_op jit(solution)/shard_map/combine/pallas_call | solution.py:300
  147.1 1.1 convolution_convert_fusion.5
  148.2 0.2 fusion.29
  148.5 0.5 slice.46
  (41 shorter events, 1.5 us)
Async XLA Ops:
  0.6 90.7 %copy-start = (bf16[1,2048,768]{2,1,0:T(8,128)(2,1)S(1)}, bf16[1,2048,768]{2,1,0:T(8,128)(2,1)}, u32[]{:S(2)}) copy-start(bf16[1,2048,768]{2,1,0:T(8,128)(2,1)} %param.12) | copy-start | bytes 9437188
  0.6 23.1 %copy-start.3 = (s32[128,2]{0,1:T(2,128)S(1)}, s32[128,2]{0,1:T(2,128)}, u32[]{:S(2)}) copy-start(s32[128,2]{0,1:T(2,128)} %param.10) | copy-start | bytes 3076
  16.5 7.3 %copy-start.2 = (f32[32,4,128]{2,1,0:T(4,128)S(1)}, f32[32,4,128]{2,1,0:T(4,128)}, u32[]{:S(2)}) copy-start(f32[32,4,128]{2,1,0:T(4,128)} %get-tuple-element.11) | copy-start | bytes 196612
  19.6 13.0 %all-to-all-start = ((bf16[4,128,512]{2,1,0:T(8,128)(2,1)}), bf16[4,128,512]{2,1,0:T(8,128)(2,1)}, u32[]{:S(2)}, u32[]{:S(2)}) async-start(bf16[4,128,512]{2,1,0:T(8,128)(2,1)} %bitcast.116), calls=%async_computation | async-start | bytes 1048576 | tf_op jit(solution)/shard_map/all_to_all | solution.py:357
  36.1 1.1 copy-start.1
  91.4 1.9 %copy-start.4 = (bf16[1,768,2048]{2,1,0:T(8,128)(2,1)S(1)}, bf16[1,768,2048]{2,1,0:T(8,128)(2,1)}, u32[]{:S(2)}) copy-start(bf16[1,768,2048]{2,1,0:T(8,128)(2,1)} %param.14) | copy-start | bytes 9437188
  104.8 3.7 %copy-start.5 = (bf16[1,2048,768]{2,1,0:T(8,128)(2,1)S(1)}, bf16[1,2048,768]{2,1,0:T(8,128)(2,1)}, u32[]{:S(2)}) copy-start(bf16[1,2048,768]{2,1,0:T(8,128)(2,1)} %param.13) | copy-start | bytes 9437188

commit v3 on v2

--- a/solution.py
+++ b/solution.py
@@ -67,12 +67,14 @@
 
 
 def dispatch_kernel(
-    plane_size, slots, tok_ref, cot_ref, sel_ref, tok_out, cot_out,
-    zbuf, sbuf, zs_sem, zr_sem, ps_sem, pr_sem, loc_sem,
+    plane_size, slots, tok_ref, sel_ref, pack_ref, moe_ref, grad_ref, gain_ref, coef_ref, tok_out, cot_out,
+    cot_part, cot_rows, cot_send, zbuf, sbuf, ts_sem, tr_sem, zs_sem, zr_sem, ps_sem, pr_sem, loc_sem,
 ):
     z, own, z_count, z_peer, plane_peer = places(plane_size)
-    features = tok_ref.shape[-1]
-    sends, outs = (tok_ref, cot_ref), (tok_out, cot_out)
+    x, t = lax.axis_index("x"), lax.axis_index("tp")
+    t_count, part_rows, part_cols = cot_rows.shape
+    group_rows, features = tok_ref.shape[1:]
+    sends, outs = (tok_ref, cot_send), (tok_out, cot_out)
     enter(z_count, plane_size, z_peer, plane_peer)
 
     def z_copy(a, d):
@@ -106,13 +108,18 @@
             sbuf.at[a, d, rows_of(own)], outs[a].at[src, rows_of(own)], loc_sem.at[a, d]
         )
 
-    for a in range(2):
-        for d in range(1, z_count):
-            z_copy(a, d).start()
-    for a, d in [(0, 0), (1, 0)] + [(a, d) for a in range(2) for d in range(1, z_count)]:
+    def part_copy(j):
+        return pltpu.make_async_remote_copy(
+            src_ref=cot_part.at[j],
+            dst_ref=cot_rows.at[t],
+            send_sem=ts_sem.at[j],
+            recv_sem=tr_sem.at[j],
+            device_id=(z, x, lax.rem(t + j, t_count)),
+            device_id_type=MESH,
+        )
+
+    def spread_block(a, d):
         src = lax.rem(z + z_count - d, z_count)
-        if d:
-            z_copy(a, d).wait_recv()
 
         def read(cols):
             return zbuf[a, d, :, cols] if d else sends[a][z, :, cols]
@@ -123,6 +130,47 @@
         columns_dot(sel_ref[src], read, write, features)
         lax.fori_loop(1, plane_size, lambda k, c: (plane_copy(a, d, k).start(), c)[1], 0)
         own_copy(a, d).start()
+
+    for d in range(1, z_count):
+        z_copy(0, d).start()
+    block = 32
+    for j in list(range(1, t_count)) + [0]:
+        first = lax.rem(t + j, t_count) * part_rows
+
+        def norm_rows(i, carry):
+            rows = pl.ds(pl.multiple_of(first + i * block, block), block)
+            scaled = gain_ref[...] * grad_ref[rows, :].astype(jnp.float32)
+            saved_out = moe_ref[rows, :].astype(jnp.float32)
+            value = coef_ref[rows, 0:1] * scaled - saved_out * coef_ref[rows, 1:2]
+            here = pl.ds(pl.multiple_of(i * block, block), block)
+            if j:
+                cot_part[j, here, :] = value.astype(cot_part.dtype)
+            else:
+                cot_rows[t, here, :] = value.astype(cot_rows.dtype)
+            return carry
+
+        lax.fori_loop(0, part_rows // block, norm_rows, 0)
+        if j:
+            part_copy(j).start()
+    spread_block(0, 0)
+    for j in range(1, t_count):
+        part_copy(j).wait_recv()
+    for part in range(t_count):
+        packed = jnp.dot(pack_ref[...], cot_rows[part], preferred_element_type=jnp.float32)
+        packed = packed.astype(cot_send.dtype)
+        for g in range(z_count):
+            cot_send[g, :, part * part_cols : (part + 1) * part_cols] = packed[
+                g * group_rows : (g + 1) * group_rows
+            ]
+    for d in range(1, z_count):
+        z_copy(1, d).start()
+    spread_block(1, 0)
+    for a in range(2):
+        for d in range(1, z_count):
+            z_copy(a, d).wait_recv()
+            spread_block(a, d)
+    for j in range(1, t_count):
+        part_copy(j).wait_send()
     for a in range(2):
         for d in range(z_count):
             if d:
@@ -266,19 +314,26 @@
     )(stats, meta)
 
 
-def dispatch(tok_send, cot_send, select, plane_size, slots):
+def dispatch(tok_send, select, pack, moe_out, out_grad, gain, coefs, plane_size, slots):
     z_count, rows, features = tok_send.shape
+    t_count = lax.axis_size("tp")
+    part = (t_count, moe_out.shape[0] // t_count, moe_out.shape[1])
     out = jax.ShapeDtypeStruct((z_count, plane_size * slots, features), tok_send.dtype)
     vmem, any_space = pl.BlockSpec(memory_space=pltpu.VMEM), pl.BlockSpec(memory_space=pl.ANY)
     dma = pltpu.SemaphoreType.DMA
     return pl.pallas_call(
         functools.partial(dispatch_kernel, plane_size, slots),
         out_shape=(out, out),
-        in_specs=[vmem] * 3,
+        in_specs=[vmem] * 7,
         out_specs=(any_space, any_space),
         scratch_shapes=[
+            pltpu.VMEM(part, tok_send.dtype),
+            pltpu.VMEM(part, tok_send.dtype),
+            pltpu.VMEM(tok_send.shape, tok_send.dtype),
             pltpu.VMEM((2, z_count, rows, features), tok_send.dtype),
             pltpu.VMEM((2,) + out.shape, tok_send.dtype),
+            dma((t_count,)),
+            dma((t_count,)),
             dma((2, z_count)),
             dma((2, z_count)),
             dma((2, z_count, plane_size)),
@@ -289,7 +344,7 @@
             collective_id=0, has_side_effects=True, vmem_limit_bytes=48 * 1024 * 1024
         ),
         name="dispatch",
-    )(tok_send, cot_send, select)
+    )(tok_send, select, pack, moe_out, out_grad, gain, coefs)
 
 
 def combine(back, gate_back, comb, plane_size, slots):
@@ -351,16 +406,12 @@
     all_gates = lax.reduce_precision(all_meta[:, route_count:], 8, 7)
 
     inv_rms = lax.rsqrt(square_sum / features + epsilon)
-    expert_cot = (
-        inv_rms[:, None] * scaled - saved_out * (inv_rms**3 * cross_sum / features)[:, None]
-    ).astype(bf16)
-    cot_rows = lax.all_to_all(expert_cot, "tp", split_axis=0, concat_axis=1, tiled=True)
+    coefs = jnp.stack([inv_rms, inv_rms**3 * cross_sum / features], axis=1)
 
     own_group = routes[:, 0] // plane_size
     z_slot = own_group * group_rows + earlier_equal(own_group)
     pack = (jnp.arange(groups * group_rows, dtype=jnp.int32)[:, None] == z_slot[None, :]).astype(bf16)
     tok_send = jnp.dot(pack, tokens, preferred_element_type=jnp.float32).astype(bf16)
-    cot_send = jnp.dot(pack, cot_rows, preferred_element_type=jnp.float32).astype(bf16)
 
     ids = lax.dynamic_index_in_dim(
         all_ids.reshape(z_count, plane_size, route_count), own, axis=1, keepdims=False
@@ -388,8 +439,12 @@
 
     token_in, cot_in = dispatch(
         tok_send.reshape(groups, group_rows, features),
-        cot_send.reshape(groups, group_rows, features),
         select,
+        pack,
+        moe_out,
+        out_grad,
+        norm_gain[None, :],
+        coefs,
         plane_size,
         slots,
     )

time: 150 us -> 155 us (1.033)
  matrix products: 28 us -> 34.3 us
  starting transfers between devices: 4.13 us -> 0 us
  local copies, waits for them, and re-layouts: 4.9 us -> 8.88 us
  waiting for transfers between devices: 2.97 us -> 0 us
  Pallas kernels: 98.6 us -> 101 us
    pallas_call x1, Pallas kernels: 50.5 us -> 57 us  [dispatch(): pl.pallas_call(functools.partial(dispatch_kernel, plane_size, slots), out...]
    unnamed x16 -> x52, local copies, waits for them, and re-layouts: 1.26 us -> 7.14 us
    dot_general x8, matrix products: 18.4 us -> 23 us  [contract(): lax.dot_general(left, right, (((left_dim,), (right_dim,)), ((), ())), pre...]
    pallas_call x1, Pallas kernels: 36.5 us -> 32.2 us  [combine(): pl.pallas_call(functools.partial(combine_kernel, plane_size, slots), out_...]
    all_to_all x1 -> x0, starting transfers between devices: 4.13 us -> none  [local(): lax.all_to_all(expert_cot, 'tp', split_axis=0, concat_axis=1, tiled=True)]
    all_to_all x1 -> x0, waiting for transfers between devices: 2.97 us -> none  [local(): lax.all_to_all(expert_cot, 'tp', split_axis=0, concat_axis=1, tiled=True)]
    all_to_all x1 -> x0, local copies, waits for them, and re-layouts: 2.04 us -> none  [local(): lax.all_to_all(expert_cot, 'tp', split_axis=0, concat_axis=1, tiled=True)]
    dot_general x1, matrix products: 3.67 us -> 5.58 us  [local(): pre_up = jnp.dot(row_block, w_up_one, preferred_element_type=jnp.float32)]
  transfers between devices with their start and end apart: 1 -> 0, of which waited for: 1 -> 0; matrix products, arithmetic and copies ran while one was open for 4% -> 0% of each run, Pallas kernels for 0% -> 0%
where the time goes in v3:
time: 155 us; the launch traced here: 154 us
  Pallas kernels  101 us (65%)
  matrix products  34.3 us (22%)
  other arithmetic  9.11 us (6%)
  local copies, waits for them, and re-layouts  8.88 us (6%)
    pallas_call x1, Pallas kernels, dispatch(): pl.pallas_call(functools.partial(dispatch_kernel, plane_size, slots), out...  57 us
    pallas_call x1, Pallas kernels, combine(): pl.pallas_call(functools.partial(combine_kernel, plane_size, slots), out_...  32.2 us
    dot_general x8, matrix products, contract(): lax.dot_general(left, right, (((left_dim,), (right_dim,)), ((), ())), pre...  23 us
    pallas_call x1, Pallas kernels, share(): pl.pallas_call(functools.partial(share_kernel, devices), out_shape=(jax.S...  11.6 us
    unnamed x52, local copies, waits for them, and re-layouts  7.14 us
    dot_general x1, matrix products, local(): pre_up = jnp.dot(row_block, w_up_one, preferred_element_type=jnp.float32)  5.58 us

profile of v3, /device:TPU:0, one launch (start us, length us, event | category | flops | bytes accessed | tf_op | source)
XLA Modules:
  0.0 154.1 jit_solution(16171996387080847963)
XLA Ops:
  0.7 0.8 and_select_fusion.2
  1.5 0.8 fusion.43
  2.5 0.7 multiply_add_fusion
  3.2 2.3 %convolution_convert_fusion.3 = bf16[192,2048]{1,0:T(8,128)(2,1)} fusion(bf16[128,2048]{1,0:T(8,128)(2,1)} %param.9, s32[128]{0:T(128)S(1)} %multiply_add_fusion), kind=kOutput, calls=%fused_computation.18 | convolution fusion | flops 101081088 | bytes 1311232 | tf_op jit(solution)/shard_map/dot_general | solution.py:414
  5.5 1.5 fusion.17
  7.0 0.6 reshape.224.stat_ref
  7.6 0.6 pad_maximum_fusion.2.meta_ref
  8.2 11.6 %share.1 = (f32[4,8,128]{2,1,0:T(8,128)}, f32[32,4,128]{2,1,0:T(4,128)}) custom-call(f32[8,128]{1,0:T(8,128)} %reshape.224.stat_ref, f32[4,128]{1,0:T(4,128)} %pad_maximum_fusion.2.meta_ref), custom_call_target="tpu_custom_call" | custom-call | tf_op jit(solution)/shard_map/share/pallas_call | solution.py:303
  19.9 0.8 copy.53
  20.7 0.6 slice_reduce-precision_fusion
  22.5 0.6 fusion.28.pack_ref
  23.1 0.7 reduce_sum.90
  24.1 1.1 copy-done.1
  25.2 1.0 copy-done.3
  26.3 1.0 copy-done.4
  27.3 0.8 copy-done.5
  28.1 57.0 %dispatch.1 = (bf16[4,128,2048]{2,1,0:T(8,128)(2,1)S(1)}, bf16[4,128,2048]{2,1,0:T(8,128)(2,1)}) custom-call(bf16[4,48,2048]{2,1,0:T(8,128)(2,1)S(1)} %bitcast.96, bf16[4,128,48]{2,1,0:T(8,128)(2,1)S(1)} %copy.40.sel_ref, bf16[192,128]{1,0:T(8,128)(2,1)S(1)} %copy-done.5, bf16[512,512]{1,0:T(8,128)(2,1)S(1)} %copy-done.3, bf16[512,512]{1,0:T(8,128)(2,1)S(1)} %copy-done.4, ...), custom_call_target="tpu_custom_call" | custom-call | tf_op jit(solution)/shard_map/dispatch/pallas_call | solution.py:324
  85.1 5.6 %fusion.6 = f32[512,768]{1,0:T(8,128)} fusion(bf16[512,2048]{1,0:T(8,128)(2,1)S(1)} %bitcast.100, bf16[1,2048,768]{2,1,0:T(8,128)(2,1)} %param.13), kind=kOutput, calls=%fused_computation.11 | convolution fusion | flops 1610612736 | bytes 6815744 | tf_op jit(solution)/shard_map/dot_general | solution.py:457
  90.7 3.0 %fusion.2 = f32[512,768]{1,0:T(8,128)} fusion(bf16[512,2048]{1,0:T(8,128)(2,1)S(1)} %bitcast.101, bf16[1,2048,768]{2,1,0:T(8,128)(2,1)S(1)} %copy-done), kind=kOutput, calls=%fused_computation.7 | convolution fusion | flops 1610612736 | bytes 6815744 | tf_op jit(solution)/shard_map/dot_general | solution.py:456
  93.7 0.6 reduce-window.6
  94.9 5.9 %multiply_reduce_fusion = (bf16[512]{0:T(512)(128)(2,1)S(1)}, bf16[512,768]{1,0:T(8,128)(2,1)S(1)}, bf16[512,768]{1,0:T(8,128)(2,1)S(1)}) fusion(f32[512,768]{1,0:T(8,128)} %fusion.6, f32[512,768]{1,0:T(8,128)} %fusion.2, f32[512]{0:T(512)S(1)} %mul.98, bf16[512,2048]{1,0:T(8,128)(2,1)} %bitcast.121, bf16[1,768,2048]{2,1,0:T(8,128)(2,1)} %param.14), kind=kOutput, calls=%fused_computation.21 | convolution fusion | flops 1617296896 | bytes 9964544 | tf_op jit(solution)/shard_map/dot_general | solution.py:18
  100.9 1.8 %fusion = f32[512,2048]{1,0:T(8,128)S(1)} fusion(bf16[512,768]{1,0:T(8,128)(2,1)S(1)} %get-tuple-element.22, bf16[1,2048,768]{2,1,0:T(8,128)(2,1)S(1)} %copy-done), kind=kOutput, calls=%fused_computation.5 | convolution fusion | flops 1610612736 | bytes 8126464 | tf_op jit(solution)/shard_map/dot_general | solution.py:18
  102.7 0.6 copy-done.16
  103.3 3.1 %add_convert_fusion = bf16[512,2048]{1,0:T(8,128)(2,1)} fusion(f32[512,2048]{1,0:T(8,128)S(1)} %fusion, bf16[512,768]{1,0:T(8,128)(2,1)S(1)} %get-tuple-element.23, bf16[1,2048,768]{2,1,0:T(8,128)(2,1)S(1)} %copy-done.16), kind=kOutput, calls=%fused_computation.1 | convolution fusion | flops 1612709888 | bytes 10223616 | tf_op jit(solution)/shard_map/dot_general | solution.py:18
  106.5 0.6 select_reduce_fusion
  107.6 1.6 %copy-done.2 = bf16[512,2048]{1,0:T(8,128)(2,1)S(1)} copy-done((bf16[512,2048]{1,0:T(8,128)(2,1)S(1)}, bf16[512,2048]{1,0:T(8,128)(2,1)}, u32[]{:S(2)}) %copy-start.2) | copy-done | bytes 2097176
  109.2 32.2 %combine.1 = (bf16[4,48,2048]{2,1,0:T(8,128)(2,1)S(1)}, bf16[4,48,128]{2,1,0:T(8,128)(2,1)S(1)}) custom-call(bf16[4,128,2048]{2,1,0:T(8,128)(2,1)S(1)} %bitcast.97, bf16[4,128,128]{2,1,0:T(8,128)(2,1)S(1)} %fusion.24.gate_ref, bf16[4,48,128]{2,1,0:T(8,128)(2,1)S(1)} %convolution_convert_fusion.5.comb_ref), custom_call_target="tpu_custom_call" | custom-call | tf_op jit(solution)/shard_map/combine/pallas_call | solution.py:355
  141.5 1.1 convolution_convert_fusion.4
  142.9 0.5 slice.46
  143.4 3.5 %fusion.10 = bf16[1,2048,768]{2,1,0:T(8,128)(2,1)} fusion(bf16[512,2048]{1,0:T(8,128)(2,1)S(1)} %bitcast.102, bf16[512,768]{1,0:T(8,128)(2,1)S(1)} %copy-done.21), kind=kOutput, calls=%fused_computation.15 | convolution fusion | flops 1612185600 | bytes 6029312 | tf_op jit(solution)/shard_map/dot_general | solution.py:18
  146.9 3.5 %fusion.11 = bf16[1,2048,768]{2,1,0:T(8,128)(2,1)} fusion(bf16[512,2048]{1,0:T(8,128)(2,1)S(1)} %bitcast.103, bf16[512,768]{1,0:T(8,128)(2,1)S(1)} %copy-done.19), kind=kOutput, calls=%fused_computation.16 | convolution fusion | flops 1612185600 | bytes 6029312 | tf_op jit(solution)/shard_map/dot_general | solution.py:18
  150.4 3.7 %fusion.12 = bf16[1,768,2048]{2,1,0:T(8,128)(2,1)} fusion(bf16[512,2048]{1,0:T(8,128)(2,1)S(1)} %bitcast.122, f32[512]{0:T(512)S(1)} %mul.98, f32[512,768]{1,0:T(8,128)S(1)} %copy-done.22, f32[512,768]{1,0:T(8,128)S(1)} %copy-done.23), kind=kOutput, calls=%fused_computation.17 | convolution fusion | flops 1617690624 | bytes 8390656 | tf_op jit(solution)/shard_map/dot_general | solution.py:18
  (75 shorter events, 2.8 us)
Async XLA Ops:
  0.6 90.1 %copy-start = (bf16[1,2048,768]{2,1,0:T(8,128)(2,1)S(1)}, bf16[1,2048,768]{2,1,0:T(8,128)(2,1)}, u32[]{:S(2)}) copy-start(bf16[1,2048,768]{2,1,0:T(8,128)(2,1)} %param.12) | copy-start | bytes 9437188
  0.6 7.0 %copy-start.14 = (s32[128,2]{0,1:T(2,128)S(1)}, s32[128,2]{0,1:T(2,128)}, u32[]{:S(2)}) copy-start(s32[128,2]{0,1:T(2,128)} %param.10) | copy-start | bytes 3076
  0.7 23.4 %copy-start.6 = (f32[512]{0:T(512)S(1)}, f32[512]{0:T(512)}, u32[]{:S(2)}) copy-start(f32[512]{0:T(512)} %param.16) | copy-start | bytes 6148
  0.7 7.0 %copy-start.15 = (f32[128,2]{0,1:T(2,128)S(1)}, f32[128,2]{0,1:T(2,128)}, u32[]{:S(2)}) copy-start(f32[128,2]{0,1:T(2,128)} %param.11) | copy-start | bytes 3076
  20.7 3.2 %copy-start.9 = (f32[4,8,4,128]{3,1,2,0:T(8,128)}, f32[4,8,4,128]{3,1,2,0:T(8,128)S(1)}, u32[]{:S(2)}) copy-start(f32[4,8,4,128]{3,1,2,0:T(8,128)S(1)} %copy.53) | copy-start | bytes 196612
  22.1 1.7 %copy-start.12 = (s32[1,4,2,128]{3,1,2,0:T(4,128)}, s32[1,4,2,128]{3,1,2,0:T(4,128)S(1)}, u32[]{:S(2)}) copy-start(s32[1,4,2,128]{3,1,2,0:T(4,128)S(1)} %copy.55) | copy-start | bytes 12292
  24.1 1.1 copy-start.1
  25.2 1.0 copy-start.3
  26.3 1.0 copy-start.4
  27.3 0.8 copy-start.5
  85.1 5.6 %copy-start.7 = (bf16[4,128,2048]{2,1,0:T(8,128)(2,1)}, bf16[4,128,2048]{2,1,0:T(8,128)(2,1)S(1)}, u32[]{:S(2)}) copy-start(bf16[4,128,2048]{2,1,0:T(8,128)(2,1)S(1)} %get-tuple-element.14) | copy-start | bytes 6291460
  90.7 3.0 %copy-start.10 = (f32[4,8,4,128]{3,1,2,0:T(8,128)S(1)}, f32[4,8,4,128]{3,1,2,0:T(8,128)}, u32[]{:S(2)}) copy-start(f32[4,8,4,128]{3,1,2,0:T(8,128)} %copy-done.9) | copy-start | bytes 196612
  90.7 3.9 %copy-start.11 = (f32[32,256]{1,0:T(8,128)S(1)}, f32[32,256]{1,0:T(8,128)}, u32[]{:S(2)}) copy-start(f32[32,256]{1,0:T(8,128)} %get-tuple-element.24) | copy-start | bytes 98308
  100.8 1.9 %copy-start.20 = (bf16[512,768]{1,0:T(8,128)(2,1)}, bf16[512,768]{1,0:T(8,128)(2,1)S(1)}, u32[]{:S(2)}) copy-start(bf16[512,768]{1,0:T(8,128)(2,1)S(1)} %get-tuple-element.22) | copy-start | bytes 2359300
  100.9 1.9 %copy-start.18 = (bf16[512,768]{1,0:T(8,128)(2,1)}, bf16[512,768]{1,0:T(8,128)(2,1)S(1)}, u32[]{:S(2)}) copy-start(bf16[512,768]{1,0:T(8,128)(2,1)S(1)} %get-tuple-element.23) | copy-start | bytes 2359300
  100.9 2.5 %copy-start.16 = (bf16[1,2048,768]{2,1,0:T(8,128)(2,1)S(1)}, bf16[1,2048,768]{2,1,0:T(8,128)(2,1)}, u32[]{:S(2)}) copy-start(bf16[1,2048,768]{2,1,0:T(8,128)(2,1)} %param.13) | copy-start | bytes 9437188
  103.3 4.1 %copy-start.13 = (s32[1,4,2,128]{3,1,2,0:T(4,128)S(1)}, s32[1,4,2,128]{3,1,2,0:T(4,128)}, u32[]{:S(2)}) copy-start(s32[1,4,2,128]{3,1,2,0:T(4,128)} %copy-done.12) | copy-start | bytes 12292
  107.6 1.6 %copy-start.2 = (bf16[512,2048]{1,0:T(8,128)(2,1)S(1)}, bf16[512,2048]{1,0:T(8,128)(2,1)}, u32[]{:S(2)}) copy-start(bf16[512,2048]{1,0:T(8,128)(2,1)} %add_convert_fusion) | copy-start | bytes 6291460
  109.2 34.1 %copy-start.8 = (bf16[4,128,2048]{2,1,0:T(8,128)(2,1)S(1)}, bf16[4,128,2048]{2,1,0:T(8,128)(2,1)}, u32[]{:S(2)}) copy-start(bf16[4,128,2048]{2,1,0:T(8,128)(2,1)} %copy-done.7) | copy-start | bytes 6291460
  109.2 34.1 %copy-start.21 = (bf16[512,768]{1,0:T(8,128)(2,1)S(1)}, bf16[512,768]{1,0:T(8,128)(2,1)}, u32[]{:S(2)}) copy-start(bf16[512,768]{1,0:T(8,128)(2,1)} %copy-done.20) | copy-start | bytes 2359300
  143.4 3.5 %copy-start.19 = (bf16[512,768]{1,0:T(8,128)(2,1)S(1)}, bf16[512,768]{1,0:T(8,128)(2,1)}, u32[]{:S(2)}) copy-start(bf16[512,768]{1,0:T(8,128)(2,1)} %copy-done.18) | copy-start | bytes 2359300
  146.9 3.5 %copy-start.17 = (bf16[4,128,2048]{2,1,0:T(8,128)(2,1)S(1)}, bf16[4,128,2048]{2,1,0:T(8,128)(2,1)}, u32[]{:S(2)}) copy-start(bf16[4,128,2048]{2,1,0:T(8,128)(2,1)} %get-tuple-element.13) | copy-start | bytes 6291460
  146.9 3.5 %copy-start.22 = (f32[512,768]{1,0:T(8,128)S(1)}, f32[512,768]{1,0:T(8,128)}, u32[]{:S(2)}) copy-start(f32[512,768]{1,0:T(8,128)} %fusion.6) | copy-start | bytes 4718596
  146.9 3.5 %copy-start.23 = (f32[512,768]{1,0:T(8,128)S(1)}, f32[512,768]{1,0:T(8,128)}, u32[]{:S(2)}) copy-start(f32[512,768]{1,0:T(8,128)} %fusion.2) | copy-start | bytes 4718596

commit v4 on v3

--- a/solution.py
+++ b/solution.py
@@ -133,6 +133,7 @@
 
     for d in range(1, z_count):
         z_copy(0, d).start()
+    spread_block(0, 0)
     block = 32
     for j in list(range(1, t_count)) + [0]:
         first = lax.rem(t + j, t_count) * part_rows
@@ -152,7 +153,8 @@
         lax.fori_loop(0, part_rows // block, norm_rows, 0)
         if j:
             part_copy(j).start()
-    spread_block(0, 0)
+    z_copy(0, 1).wait_recv()
+    spread_block(0, 1)
     for j in range(1, t_count):
         part_copy(j).wait_recv()
     for part in range(t_count):
@@ -166,7 +168,7 @@
         z_copy(1, d).start()
     spread_block(1, 0)
     for a in range(2):
-        for d in range(1, z_count):
+        for d in range(2 - a, z_count):
             z_copy(a, d).wait_recv()
             spread_block(a, d)
     for j in range(1, t_count):
@@ -309,9 +311,21 @@
         in_specs=[vmem] * 2,
         out_specs=(vmem, vmem),
         scratch_shapes=[dma((t_count,)), dma((t_count,)), dma((devices,)), dma((devices,))],
-        compiler_params=pltpu.CompilerParams(collective_id=2, has_side_effects=True),
+        compiler_params=pltpu.CompilerParams(
+            collective_id=2, has_side_effects=True, vmem_limit_bytes=8 * 1024 * 1024
+        ),
         name="share",
     )(stats, meta)
+
+
+def grant(*arrays):
+    total = 0
+    for shape, item in arrays:
+        size = item
+        for extent in shape[:-1] + (max(shape[-1], 128),):
+            size *= extent
+        total += size
+    return total + 6 * 1024 * 1024
 
 
 def dispatch(tok_send, select, pack, moe_out, out_grad, gain, coefs, plane_size, slots):
@@ -321,6 +335,9 @@
     out = jax.ShapeDtypeStruct((z_count, plane_size * slots, features), tok_send.dtype)
     vmem, any_space = pl.BlockSpec(memory_space=pltpu.VMEM), pl.BlockSpec(memory_space=pl.ANY)
     dma = pltpu.SemaphoreType.DMA
+    limit = grant(
+        (out.shape, 4), (tok_send.shape, 8), (part, 8), (select.shape, 2), (pack.shape, 2), (coefs.shape, 4)
+    )
     return pl.pallas_call(
         functools.partial(dispatch_kernel, plane_size, slots),
         out_shape=(out, out),
@@ -341,7 +358,7 @@
             dma((2, z_count)),
         ],
         compiler_params=pltpu.CompilerParams(
-            collective_id=0, has_side_effects=True, vmem_limit_bytes=48 * 1024 * 1024
+            collective_id=0, has_side_effects=True, vmem_limit_bytes=limit
         ),
         name="dispatch",
     )(tok_send, select, pack, moe_out, out_grad, gain, coefs)
@@ -352,6 +369,7 @@
     rows, lanes = comb.shape[1], gate_back.shape[-1]
     vmem, any_space = pl.BlockSpec(memory_space=pltpu.VMEM), pl.BlockSpec(memory_space=pl.ANY)
     dma = pltpu.SemaphoreType.DMA
+    limit = grant((back.shape, 2), (gate_back.shape, 2), ((z_count, rows, features + lanes), 2), (comb.shape, 2))
     return pl.pallas_call(
         functools.partial(combine_kernel, plane_size, slots),
         out_shape=(
@@ -373,7 +391,7 @@
             dma((2,)),
         ],
         compiler_params=pltpu.CompilerParams(
-            collective_id=1, has_side_effects=True, vmem_limit_bytes=48 * 1024 * 1024
+            collective_id=1, has_side_effects=True, vmem_limit_bytes=limit
         ),
         name="combine",
     )(back, gate_back, comb)

time: 155 us -> 151 us (0.974)
    unnamed x52 -> x54, local copies, waits for them, and re-layouts: 7.14 us -> 6.31 us
where the time goes in v4:
time: 151 us
  Pallas kernels  99.5 us (66%)
  matrix products  35.1 us (23%)
  other arithmetic  7.8 us (5%)
  local copies, waits for them, and re-layouts  7.46 us (5%)
    pallas_call x1, Pallas kernels, dispatch(): pl.pallas_call(functools.partial(dispatch_kernel, plane_size, slots), out...  57.1 us
    pallas_call x1, Pallas kernels, combine(): pl.pallas_call(functools.partial(combine_kernel, plane_size, slots), out_...  31.7 us
    dot_general x8, matrix products, contract(): lax.dot_general(left, right, (((left_dim,), (right_dim,)), ((), ())), pre...  23 us
    pallas_call x1, Pallas kernels, share(): pl.pallas_call(functools.partial(share_kernel, devices), out_shape=(jax.S...  10.7 us
    dot_general x1, matrix products, local(): pre_up = jnp.dot(row_block, w_up_one, preferred_element_type=jnp.float32)  6.36 us
    unnamed x54, local copies, waits for them, and re-layouts  6.31 us

profile of v4, /device:TPU:0, one launch (start us, length us, event | category | flops | bytes accessed | tf_op | source)
XLA Modules:
  0.0 150.9 jit_solution(16634099651952925545)
XLA Ops:
  0.7 0.8 and_select_fusion.2
  1.5 0.8 fusion.43
  2.5 0.7 multiply_add_fusion
  3.2 2.3 %convolution_convert_fusion.3 = bf16[192,2048]{1,0:T(8,128)(2,1)} fusion(bf16[128,2048]{1,0:T(8,128)(2,1)} %param.9, s32[128]{0:T(128)S(1)} %multiply_add_fusion), kind=kOutput, calls=%fused_computation.18 | convolution fusion | flops 101081088 | bytes 1311232 | tf_op jit(solution)/shard_map/dot_general | solution.py:432
  5.5 1.5 %fusion.17 = (f32[512]{0:T(512)S(1)}, f32[512]{0:T(512)S(1)}) fusion(bf16[512,512]{1,0:T(8,128)(2,1)} %moe_ref.1, bf16[512,512]{1,0:T(8,128)(2,1)} %grad_ref.1, f32[512]{0:T(512)} %param.16), kind=kLoop, calls=%fused_computation.30 | loop fusion | flops 1833984 | bytes 1054720 | tf_op jit(solution)/shard_map/reduce_sum | solution.py:418
  7.1 10.7 %share.1 = (f32[4,8,128]{2,1,0:T(8,128)S(1)}, f32[32,4,128]{2,1,0:T(4,128)S(1)}) custom-call(f32[8,128]{1,0:T(8,128)S(1)} %reshape.224.stat_ref, f32[4,128]{1,0:T(4,128)S(1)} %pad_maximum_fusion.2.meta_ref), custom_call_target="tpu_custom_call" | custom-call | tf_op jit(solution)/shard_map/share/pallas_call | solution.py:305
  17.9 0.6 slice_reduce-precision_fusion
  18.5 0.4 convert_reduce_fusion
  19.0 0.2 convert_reduce_fusion.1
  19.3 0.2 convolution_convert_fusion.6
  19.6 0.6 fusion.28.pack_ref
  20.5 1.1 copy-done.1
  21.6 1.0 copy-done.3
  22.7 1.0 copy-done.4
  23.7 0.8 copy-done.5
  24.5 57.1 %dispatch.1 = (bf16[4,128,2048]{2,1,0:T(8,128)(2,1)S(1)}, bf16[4,128,2048]{2,1,0:T(8,128)(2,1)S(1)}) custom-call(bf16[4,48,2048]{2,1,0:T(8,128)(2,1)S(1)} %bitcast.96, bf16[4,128,48]{2,1,0:T(8,128)(2,1)S(1)} %copy.40.sel_ref, bf16[192,128]{1,0:T(8,128)(2,1)S(1)} %copy-done.5, bf16[512,512]{1,0:T(8,128)(2,1)S(1)} %copy-done.3, ...), custom_call_target="tpu_custom_call" | custom-call | tf_op jit(solution)/shard_map/dispatch/pallas_call | solution.py:341
  81.7 6.4 %fusion.6 = f32[512,768]{1,0:T(8,128)} fusion(bf16[512,2048]{1,0:T(8,128)(2,1)S(1)} %bitcast.103, bf16[1,2048,768]{2,1,0:T(8,128)(2,1)} %param.13), kind=kOutput, calls=%fused_computation.11 | convolution fusion | flops 1610612736 | bytes 6815744 | tf_op jit(solution)/shard_map/dot_general | solution.py:475
  88.1 2.9 %fusion.2 = f32[512,768]{1,0:T(8,128)} fusion(bf16[512,2048]{1,0:T(8,128)(2,1)S(1)} %bitcast.104, bf16[1,2048,768]{2,1,0:T(8,128)(2,1)S(1)} %copy-done), kind=kOutput, calls=%fused_computation.7 | convolution fusion | flops 1610612736 | bytes 6815744 | tf_op jit(solution)/shard_map/dot_general | solution.py:474
  91.0 0.6 reduce-window.6
  92.2 5.9 %multiply_reduce_fusion = (bf16[512]{0:T(512)(128)(2,1)S(1)}, bf16[512,768]{1,0:T(8,128)(2,1)S(1)}, bf16[512,768]{1,0:T(8,128)(2,1)S(1)}) fusion(f32[512,768]{1,0:T(8,128)} %fusion.6, f32[512,768]{1,0:T(8,128)} %fusion.2, f32[512]{0:T(512)S(1)} %mul.98, bf16[512,2048]{1,0:T(8,128)(2,1)} %bitcast.101, bf16[1,768,2048]{2,1,0:T(8,128)(2,1)} %param.14), kind=kOutput, calls=%fused_computation.21 | convolution fusion | flops 1617296896 | bytes 9964544 | tf_op jit(solution)/shard_map/dot_general | solution.py:18
  98.2 1.8 %fusion = f32[512,2048]{1,0:T(8,128)S(1)} fusion(bf16[512,768]{1,0:T(8,128)(2,1)S(1)} %get-tuple-element.22, bf16[1,2048,768]{2,1,0:T(8,128)(2,1)S(1)} %copy-done), kind=kOutput, calls=%fused_computation.5 | convolution fusion | flops 1610612736 | bytes 8126464 | tf_op jit(solution)/shard_map/dot_general | solution.py:18
  100.0 0.6 copy-done.18
  100.7 3.1 %add_convert_fusion = bf16[512,2048]{1,0:T(8,128)(2,1)} fusion(f32[512,2048]{1,0:T(8,128)S(1)} %fusion, bf16[512,768]{1,0:T(8,128)(2,1)S(1)} %get-tuple-element.23, bf16[1,2048,768]{2,1,0:T(8,128)(2,1)S(1)} %copy-done.18), kind=kOutput, calls=%fused_computation.1 | convolution fusion | flops 1612709888 | bytes 10223616 | tf_op jit(solution)/shard_map/dot_general | solution.py:18
  103.8 0.6 select_reduce_fusion
  104.7 0.2 convolution_convert_fusion.5.comb_ref
  105.0 1.6 %copy-done.2 = bf16[512,2048]{1,0:T(8,128)(2,1)S(1)} copy-done((bf16[512,2048]{1,0:T(8,128)(2,1)S(1)}, bf16[512,2048]{1,0:T(8,128)(2,1)}, u32[]{:S(2)}) %copy-start.2) | copy-done | bytes 2097176
  106.6 31.7 %combine.1 = (bf16[4,48,2048]{2,1,0:T(8,128)(2,1)S(1)}, bf16[4,48,128]{2,1,0:T(8,128)(2,1)S(1)}) custom-call(bf16[4,128,2048]{2,1,0:T(8,128)(2,1)S(1)} %bitcast.97, bf16[4,128,128]{2,1,0:T(8,128)(2,1)S(1)} %fusion.24.gate_ref, bf16[4,48,128]{2,1,0:T(8,128)(2,1)S(1)} %convolution_convert_fusion.5.comb_ref), custom_call_target="tpu_custom_call" | custom-call | tf_op jit(solution)/shard_map/combine/pallas_call | solution.py:373
  138.2 1.2 convolution_convert_fusion.4
  139.6 0.5 slice.46
  140.1 3.5 %fusion.10 = bf16[1,2048,768]{2,1,0:T(8,128)(2,1)} fusion(bf16[512,2048]{1,0:T(8,128)(2,1)S(1)} %bitcast.105, bf16[512,768]{1,0:T(8,128)(2,1)S(1)} %copy-done.22), kind=kOutput, calls=%fused_computation.15 | convolution fusion | flops 1612185600 | bytes 6029312 | tf_op jit(solution)/shard_map/dot_general | solution.py:18
  143.7 3.5 %fusion.11 = bf16[1,2048,768]{2,1,0:T(8,128)(2,1)} fusion(bf16[512,2048]{1,0:T(8,128)(2,1)S(1)} %bitcast.106, bf16[512,768]{1,0:T(8,128)(2,1)S(1)} %copy-done.20), kind=kOutput, calls=%fused_computation.16 | convolution fusion | flops 1612185600 | bytes 6029312 | tf_op jit(solution)/shard_map/dot_general | solution.py:18
  147.2 3.7 %fusion.12 = bf16[1,768,2048]{2,1,0:T(8,128)(2,1)} fusion(bf16[512,2048]{1,0:T(8,128)(2,1)S(1)} %bitcast.102, f32[512]{0:T(512)S(1)} %mul.98, f32[512,768]{1,0:T(8,128)S(1)} %copy-done.23, f32[512,768]{1,0:T(8,128)S(1)} %copy-done.24), kind=kOutput, calls=%fused_computation.17 | convolution fusion | flops 1617690624 | bytes 8390656 | tf_op jit(solution)/shard_map/dot_general | solution.py:18
  (77 shorter events, 1.8 us)
Async XLA Ops:
  0.6 87.4 %copy-start = (bf16[1,2048,768]{2,1,0:T(8,128)(2,1)S(1)}, bf16[1,2048,768]{2,1,0:T(8,128)(2,1)}, u32[]{:S(2)}) copy-start(bf16[1,2048,768]{2,1,0:T(8,128)(2,1)} %param.12) | copy-start | bytes 9437188
  0.6 6.4 %copy-start.16 = (s32[128,2]{0,1:T(2,128)S(1)}, s32[128,2]{0,1:T(2,128)}, u32[]{:S(2)}) copy-start(s32[128,2]{0,1:T(2,128)} %param.10) | copy-start | bytes 3076
  0.7 19.8 %copy-start.6 = (f32[512]{0:T(512)S(1)}, f32[512]{0:T(512)}, u32[]{:S(2)}) copy-start(f32[512]{0:T(512)} %param.16) | copy-start | bytes 6148
  0.7 6.4 %copy-start.17 = (f32[128,2]{0,1:T(2,128)S(1)}, f32[128,2]{0,1:T(2,128)}, u32[]{:S(2)}) copy-start(f32[128,2]{0,1:T(2,128)} %param.11) | copy-start | bytes 3076
  17.8 2.5 %copy-start.11 = (f32[4,8,4,128]{3,1,2,0:T(8,128)}, f32[4,8,4,128]{3,1,2,0:T(8,128)S(1)}, u32[]{:S(2)}) copy-start(f32[4,8,4,128]{3,1,2,0:T(8,128)S(1)} %copy.53) | copy-start | bytes 196612
  19.3 1.0 copy-start.14
  20.5 1.1 copy-start.1
  21.6 1.0 copy-start.3
  22.7 1.0 copy-start.4
  23.7 0.8 copy-start.5
  81.7 6.4 %copy-start.9 = (bf16[4,128,2048]{2,1,0:T(8,128)(2,1)}, bf16[4,128,2048]{2,1,0:T(8,128)(2,1)S(1)}, u32[]{:S(2)}) copy-start(bf16[4,128,2048]{2,1,0:T(8,128)(2,1)S(1)} %get-tuple-element.14) | copy-start | bytes 6291460
  81.7 9.3 %copy-start.7 = (bf16[4,128,2048]{2,1,0:T(8,128)(2,1)}, bf16[4,128,2048]{2,1,0:T(8,128)(2,1)S(1)}, u32[]{:S(2)}) copy-start(bf16[4,128,2048]{2,1,0:T(8,128)(2,1)S(1)} %get-tuple-element.13) | copy-start | bytes 6291460
  88.1 3.0 %copy-start.12 = (f32[4,8,4,128]{3,1,2,0:T(8,128)S(1)}, f32[4,8,4,128]{3,1,2,0:T(8,128)}, u32[]{:S(2)}) copy-start(f32[4,8,4,128]{3,1,2,0:T(8,128)} %copy-done.11) | copy-start | bytes 196612
  88.1 3.9 %copy-start.13 = (f32[32,256]{1,0:T(8,128)S(1)}, f32[32,256]{1,0:T(8,128)}, u32[]{:S(2)}) copy-start(f32[32,256]{1,0:T(8,128)} %get-tuple-element.24) | copy-start | bytes 98308
  98.2 1.9 %copy-start.21 = (bf16[512,768]{1,0:T(8,128)(2,1)}, bf16[512,768]{1,0:T(8,128)(2,1)S(1)}, u32[]{:S(2)}) copy-start(bf16[512,768]{1,0:T(8,128)(2,1)S(1)} %get-tuple-element.22) | copy-start | bytes 2359300
  98.2 1.9 %copy-start.19 = (bf16[512,768]{1,0:T(8,128)(2,1)}, bf16[512,768]{1,0:T(8,128)(2,1)S(1)}, u32[]{:S(2)}) copy-start(bf16[512,768]{1,0:T(8,128)(2,1)S(1)} %get-tuple-element.23) | copy-start | bytes 2359300
  98.2 2.5 %copy-start.18 = (bf16[1,2048,768]{2,1,0:T(8,128)(2,1)S(1)}, bf16[1,2048,768]{2,1,0:T(8,128)(2,1)}, u32[]{:S(2)}) copy-start(bf16[1,2048,768]{2,1,0:T(8,128)(2,1)} %param.13) | copy-start | bytes 9437188
  100.6 4.1 %copy-start.15 = (s32[1,4,2,128]{3,1,2,0:T(4,128)S(1)}, s32[1,4,2,128]{3,1,2,0:T(4,128)}, u32[]{:S(2)}) copy-start(s32[1,4,2,128]{3,1,2,0:T(4,128)} %copy-done.14) | copy-start | bytes 12292
  105.0 1.6 %copy-start.2 = (bf16[512,2048]{1,0:T(8,128)(2,1)S(1)}, bf16[512,2048]{1,0:T(8,128)(2,1)}, u32[]{:S(2)}) copy-start(bf16[512,2048]{1,0:T(8,128)(2,1)} %add_convert_fusion) | copy-start | bytes 6291460
  106.6 33.6 %copy-start.10 = (bf16[4,128,2048]{2,1,0:T(8,128)(2,1)S(1)}, bf16[4,128,2048]{2,1,0:T(8,128)(2,1)}, u32[]{:S(2)}) copy-start(bf16[4,128,2048]{2,1,0:T(8,128)(2,1)} %copy-done.9) | copy-start | bytes 6291460
  106.6 33.6 %copy-start.22 = (bf16[512,768]{1,0:T(8,128)(2,1)S(1)}, bf16[512,768]{1,0:T(8,128)(2,1)}, u32[]{:S(2)}) copy-start(bf16[512,768]{1,0:T(8,128)(2,1)} %copy-done.21) | copy-start | bytes 2359300
  140.1 3.5 %copy-start.20 = (bf16[512,768]{1,0:T(8,128)(2,1)S(1)}, bf16[512,768]{1,0:T(8,128)(2,1)}, u32[]{:S(2)}) copy-start(bf16[512,768]{1,0:T(8,128)(2,1)} %copy-done.19) | copy-start | bytes 2359300
  143.7 3.5 %copy-start.8 = (bf16[4,128,2048]{2,1,0:T(8,128)(2,1)S(1)}, bf16[4,128,2048]{2,1,0:T(8,128)(2,1)}, u32[]{:S(2)}) copy-start(bf16[4,128,2048]{2,1,0:T(8,128)(2,1)} %copy-done.7) | copy-start | bytes 6291460
  143.7 3.5 %copy-start.23 = (f32[512,768]{1,0:T(8,128)S(1)}, f32[512,768]{1,0:T(8,128)}, u32[]{:S(2)}) copy-start(f32[512,768]{1,0:T(8,128)} %fusion.6) | copy-start | bytes 4718596
  143.7 3.5 %copy-start.24 = (f32[512,768]{1,0:T(8,128)S(1)}, f32[512,768]{1,0:T(8,128)}, u32[]{:S(2)}) copy-start(f32[512,768]{1,0:T(8,128)} %fusion.2) | copy-start | bytes 4718596
